TPU v7x, 256 devices: a 4x2x16 block of a 4x16x16 slice. The times are simulated.
256 devices in a mesh: grp: 2 (over y), ep: 32 (over z, core), tp: 4 (over x).
Axes of the slice: x: 4, y: 2, z: 16, core: 2. Of those that a mesh axis runs over, the one named last changes fastest.
The devices are a block of a 4x16x16 slice.
Arguments:
- query: bfloat16 [65536, 1024], P(('grp', 'ep'), 'tp'), parts along dimension 0, may hold values from -6 to 6
- forget_gate_logits: bfloat16 [65536, 1024], P(('grp', 'ep'), 'tp'), parts along dimension 0, may hold values from -8 to 8
- value: bfloat16 [65536, 1024], P(('grp', 'ep'), 'tp'), parts along dimension 0, may hold values from -6 to 6
- forget_lower_margin: float32 [2, 1024], P(None, 'tp'), may hold values from -30 to -2
- position_log_decay: float32 [8, 65536], P('tp', ('grp', 'ep')), parts along dimension 1, may hold values from -1.5 to 0
- head_norm_gain: float32 [128], replicated, may hold values from 0.1 to 1.9
- mixer_output_weight: bfloat16 [1024, 2048], P('tp'), may hold values from -0.1875 to 0.1875
- second_batch_tokens: bfloat16 [32768, 2048], P(('grp', 'ep', 'tp')), parts along dimension 0, may hold values from -60 to 60
- expert_norm_gain: float32 [2048], replicated, may hold values from 0.1 to 1.9
- routes: int32 [32768, 2], P(('grp', 'ep', 'tp')), parts along dimension 0, may hold values from 0 to 31, all different within a row; in each aligned block of 128 rows (0 to 127, 128 to 255, ...) at most 12 rows name the same one
- chosen_expert_weight: float32 [32768, 2], P(('grp', 'ep', 'tp')), parts along dimension 0, may hold values from 0.2 to 1
- gate_weight: bfloat16 [32, 2048, 2048], P('ep', None, 'tp'), may hold values from -0.3125 to 0.3125
- up_weight: bfloat16 [32, 2048, 2048], P('ep', None, 'tp'), may hold values from -0.3125 to 0.3125
- down_weight: bfloat16 [32, 2048, 2048], P('ep', 'tp'), may hold values from -0.02734375 to 0.02734375
Outputs:
- first_mixer_output: bfloat16 [65536, 2048], P(('grp', 'ep', 'tp')), parts along dimension 0
- moe_out: bfloat16 [32768, 2048], P(('grp', 'ep', 'tp')), parts along dimension 0
There are 2 independent parts, one for each index of `grp`. A program takes and returns all parts, laid end to end along the dimension named above; an argument that names none is the same for every part. Nothing has to cross between parts.
Inputs may be any that keep to these rules, and one draw needn't show every extreme that they name: `routes`: each row names 2 different experts. Among the rows of one device no expert is named by more than 12 rows, and in every draw some expert is named by exactly 12 rows of some device.
All inputs are finite; a program needn't handle non-finite values.
Results may differ from a plain program's by a relative error of at most 0.015.
Values may be sent and summed in bfloat16 or wider, within the bound.
A program may use at most 128 MiB of HBM per device.

v0:
```python
import jax
import jax.numpy as jnp
from jax import lax
from jax.sharding import Mesh
from jax.sharding import PartitionSpec as P

HEAD_CHANNELS = 128
BLK = 128
EP = ("ep_0", "ep_1")
GRP_EP = ("grp", "ep_0", "ep_1")
GRP_EP_TP = ("grp", "ep_0", "ep_1", "tp")


NORM_EPS = 1e-06
CLAMP_LIMIT = 7.0
SIGMOID_SCALE = 1.702


def neutral_like(value, identity):
    return jax.tree.map(
        lambda part, zero: jnp.zeros_like(part) + jnp.asarray(zero, part.dtype), value, identity
    )


def entering_2(value, axes, combine, identity, reverse):
    before = start = neutral_like(value, identity)
    so_far = value
    for axis in reversed(axes):
        length, position = (lax.axis_size(axis), lax.axis_index(axis))
        pieces = jax.tree.map(
            lambda part, kind: lax.all_gather(part.astype(kind), axis),
            so_far,
            (jnp.bfloat16, jnp.bfloat16),
        )
        inside, so_far = (start, start)
        for k in reversed(range(length)) if reverse else range(length):
            passed = k > position if reverse else k < position
            so_far = combine(
                so_far, jax.tree.map(lambda part, own: part[k].astype(own.dtype), pieces, value)
            )
            inside = jax.tree.map(lambda new, old: jnp.where(passed, new, old), so_far, inside)
        before = combine(inside, before)
    return before


def cut_along(value, dim, length):
    dims = value.shape
    pieces = value.reshape(*dims[:dim], length, dims[dim] // length, *dims[dim + 1 :])
    return jnp.moveaxis(pieces, dim, 0)


def joined_along(pieces, dim):
    dims = list(pieces.shape[1:])
    dims[dim] *= pieces.shape[0]
    return jnp.moveaxis(pieces, 0, dim).reshape(dims)


def turned_blocks(pieces, axes, order):
    inside = pieces.shape[1:]
    result = pieces.reshape(*(lax.axis_size(a) for a in axes), *inside)
    for k in order:
        result = lax.all_to_all(result, axes[k], k, k, tiled=True)
    return result.reshape(-1, *inside)


def two_step_exchange(value, groups, order, split_dim, concat_dim):
    length = lax.axis_size(groups[0]) * lax.axis_size(groups[1])
    pieces = cut_along(value, split_dim, length)
    return joined_along(turned_blocks(pieces, groups, order), concat_dim)


def sum_at_owner(value, axis, dim):
    pieces = cut_along(value, dim, lax.axis_size(axis))
    arrived = lax.all_to_all(pieces, axis, split_axis=0, concat_axis=0, tiled=True)
    return arrived.astype(jnp.float32).sum(axis=0)


def clamped_unit(gate_pre, up_pre):
    gate_pre = jnp.minimum(gate_pre, CLAMP_LIMIT)
    up_pre = jnp.clip(up_pre, -CLAMP_LIMIT, CLAMP_LIMIT)
    return (up_pre + 1.0) * gate_pre * jax.nn.sigmoid(SIGMOID_SCALE * gate_pre)


def local_recurrence(queries, ending_state, values, forget_log_rates):
    sequence_length, number_of_heads, channels = queries.shape
    nblocks = sequence_length // BLK

    def to_blocks(array):
        return array.reshape(nblocks, BLK, number_of_heads, array.shape[-1])

    query_blocks = to_blocks(queries)
    key_blocks = to_blocks(ending_state)
    value_blocks = to_blocks(values)
    cumul = jnp.cumsum(to_blocks(forget_log_rates), axis=1)
    block_last = cumul[:, -1]
    query_in = query_blocks * jnp.exp(cumul)
    key_in = key_blocks * jnp.exp(-cumul)
    key_state = key_blocks * jnp.exp(block_last[:, None] - cumul)
    lower = jnp.tril(jnp.ones((BLK, BLK), jnp.float32))
    scores = jnp.einsum("nchd,nshd->nhcs", query_in, key_in) * lower
    inner = jnp.einsum("nhcs,nshv->nchv", scores, value_blocks)
    increments = jnp.einsum("nshd,nshv->nhdv", key_state, value_blocks)

    def advance(state, inputs):
        decay, increment = inputs
        return (state * decay[..., None] + increment, state)

    initial = jnp.zeros((number_of_heads, channels, values.shape[-1]), jnp.float32)
    final_state, before = lax.scan(advance, initial, (jnp.exp(block_last), increments))
    outer = jnp.einsum("nchd,nhdv->nchv", query_in, before)
    output = (inner + outer).reshape(sequence_length, number_of_heads, values.shape[-1])
    offsets = jnp.cumsum(block_last, axis=0) - block_last
    carried_query = (query_blocks * jnp.exp(cumul + offsets[:, None])).reshape(
        sequence_length, number_of_heads, channels
    )
    total_log = jnp.sum(block_last, axis=0)
    return (output, final_state, total_log, carried_query)


def chain_combine(earlier, later):
    return (earlier[0] * later[0], earlier[1] * later[0][..., None] + later[1])


def mixer_head_states(
    query, forget_gate_logits, value, forget_lower_margin, position_log_decay, head_norm_gain
):
    sequence_length = query.shape[0]
    number_of_heads = query.shape[1] // HEAD_CHANNELS
    queries = jax.nn.silu(query.astype(jnp.float32)).reshape(
        sequence_length, number_of_heads, HEAD_CHANNELS
    ) * HEAD_CHANNELS ** (-0.5)
    values = value.astype(jnp.float32).reshape(sequence_length, number_of_heads, HEAD_CHANNELS)
    shutting = jax.nn.sigmoid(-forget_gate_logits.astype(jnp.float32))
    decay_spikes = jnp.transpose(position_log_decay)[:, :, None]
    ending_state = jnp.exp(forget_lower_margin[0])[None, :] * shutting
    forget_log_rates = (
        jnp.log1p(-ending_state).reshape(sequence_length, number_of_heads, HEAD_CHANNELS)
        + decay_spikes
    )
    ending_state = ending_state.reshape(sequence_length, number_of_heads, HEAD_CHANNELS)
    output, final_state, total_log, carried = local_recurrence(
        queries, ending_state, values, forget_log_rates
    )
    identity = (jnp.ones_like(total_log), jnp.zeros_like(final_state))
    entering = entering_2((jnp.exp(total_log), final_state), EP, chain_combine, identity, False)[1]
    forward = output + jnp.einsum("lhd,hdv->lhv", carried, entering)
    ending_state = jnp.exp(forget_lower_margin[1])[None, :] * shutting
    forget_log_rates = (
        jnp.log1p(-ending_state).reshape(sequence_length, number_of_heads, HEAD_CHANNELS)
        + decay_spikes
    )
    ending_state = ending_state.reshape(sequence_length, number_of_heads, HEAD_CHANNELS)
    output, final_state, total_log, carried = local_recurrence(
        jnp.flip(queries, 0),
        jnp.flip(ending_state, 0),
        jnp.flip(values, 0),
        jnp.flip(forget_log_rates, 0),
    )
    entering = entering_2((jnp.exp(total_log), final_state), EP, chain_combine, identity, True)[1]
    backward = jnp.flip(output + jnp.einsum("lhd,hdv->lhv", carried, entering), 0)
    mix = forward + backward
    scaled = (
        mix * lax.rsqrt(jnp.mean(mix * mix, axis=-1, keepdims=True) + NORM_EPS) * head_norm_gain
    )
    return scaled.reshape(sequence_length, number_of_heads * HEAD_CHANNELS).astype(jnp.bfloat16)


def body(
    query,
    forget_gate_logits,
    value,
    forget_lower_margin,
    position_log_decay,
    head_norm_gain,
    mixer_output_weight,
    second_batch_tokens,
    expert_norm_gain,
    routes,
    chosen_expert_weight,
    gate_weight,
    up_weight,
    down_weight,
):
    head_outputs = mixer_head_states(
        query, forget_gate_logits, value, forget_lower_margin, position_log_decay, head_norm_gain
    )
    tokens, top_count = routes.shape
    features = second_batch_tokens.shape[1]
    n_ep = lax.axis_size(EP)
    capacity = (3 * tokens * top_count + 2 * n_ep - 1) // (2 * n_ep)
    tokens_f = second_batch_tokens.astype(jnp.float32)
    normed = (
        tokens_f
        * lax.rsqrt(jnp.mean(tokens_f * tokens_f, axis=-1, keepdims=True) + NORM_EPS)
        * expert_norm_gain
    ).astype(jnp.bfloat16)
    flat_routes = routes.reshape(-1)
    onehot = (flat_routes[:, None] == jnp.arange(n_ep, dtype=jnp.int32)[None, :]).astype(jnp.int32)
    ranking = jnp.cumsum(onehot, axis=0) - onehot
    slot_index = jnp.sum(ranking * onehot, axis=1)
    destination = flat_routes * capacity + slot_index
    source = (
        jnp.full((n_ep * capacity,), tokens, jnp.int32)
        .at[destination]
        .set(jnp.arange(tokens * top_count, dtype=jnp.int32) // top_count)
    )
    padded = jnp.concatenate([normed, jnp.zeros((1, features), jnp.bfloat16)], axis=0)
    send = padded[source]
    arrived = two_step_exchange(send, ("ep_0", "ep_1"), (1, 0), 0, 0)
    piece = lax.all_gather(arrived, "tp", axis=0, tiled=True)
    gate_pre = jnp.dot(piece, gate_weight[0], preferred_element_type=jnp.float32)
    up_pre = jnp.dot(piece, up_weight[0], preferred_element_type=jnp.float32)
    hidden = clamped_unit(gate_pre, up_pre).astype(jnp.bfloat16)
    picked = head_outputs
    first_mixer_output = lax.psum_scatter(
        jnp.dot(picked, mixer_output_weight, preferred_element_type=jnp.float32).astype(
            jnp.bfloat16
        ),
        "tp",
        scatter_dimension=0,
        tiled=True,
    )
    picked = hidden
    expert_sum = sum_at_owner(
        jnp.dot(picked, down_weight[0], preferred_element_type=jnp.float32).astype(jnp.bfloat16),
        "tp",
        0,
    ).astype(jnp.bfloat16)
    returned = lax.all_to_all(expert_sum, EP, split_axis=0, concat_axis=0, tiled=True)
    gathered = returned[destination].reshape(tokens, top_count, features)
    moe_out = jnp.sum(
        chosen_expert_weight[:, :, None] * gathered.astype(jnp.float32), axis=1
    ).astype(jnp.bfloat16)
    return (first_mixer_output, moe_out)


def solution(mesh):
    finer = Mesh(
        mesh.devices.reshape(mesh.shape["grp"], 16, 2, mesh.shape["tp"]),
        ("grp", "ep_0", "ep_1", "tp"),
    )
    placed = (
        P(GRP_EP, "tp"),
        P(GRP_EP, "tp"),
        P(GRP_EP, "tp"),
        P(None, "tp"),
        P("tp", GRP_EP),
        P(),
        P("tp", None),
        P(GRP_EP_TP, None),
        P(),
        P(GRP_EP_TP, None),
        P(GRP_EP_TP, None),
        P(EP, None, "tp"),
        P(EP, None, "tp"),
        P(EP, "tp", None),
    )
    return jax.shard_map(
        body,
        mesh=finer,
        in_specs=placed,
        out_specs=(P(GRP_EP_TP, None), P(GRP_EP_TP, None)),
        check_vma=False,
    )
```

profile of v0, /device:TPU:33, one launch (start us, length us, event | category | flops | bytes accessed | tf_op | source)
XLA Modules:
  0.0 516.8 jit_solution(8012739648597230385)
XLA Ops:
  17.4 3.6 reshape_reshape.14
  23.5 25.1 %all_to_all.27 = bf16[16,2,12,2048]{3,0,2,1:T(8,128)(2,1)S(1)} all-to-all(bf16[16,2,12,2048]{3,0,2,1:T(8,128)(2,1)S(1)} %copy.158), channel_id=1, replica_groups=mesh['grp'=2,'ep_0'=16,'ep_1'=2,'tp'=4] {'ep_1'}, dimensions={1} | all-to-all | bytes 3145728 | tf_op jit(solution)/shard_map/all_to_all | solution.py:62
  50.2 72.0 %all_to_all.28 = bf16[16,2,12,2048]{3,1,2,0:T(2,128)(2,1)S(1)} all-to-all(bf16[16,2,12,2048]{3,1,2,0:T(2,128)(2,1)S(1)} %copy.159), channel_id=1, replica_groups=mesh['grp'=2,'ep_0'=16,'ep_1'=2,'tp'=4] {'ep_0'}, dimensions={0} | all-to-all | bytes 3145728 | tf_op jit(solution)/shard_map/all_to_all | solution.py:62
  124.3 3.7 reshape_reshape.15
  131.4 6.0 %rev.17 = f32[1024,2,128]{0,2,1:T(8,128)} reverse(f32[1024,2,128]{0,2,1:T(8,128)S(1)} %broadcast_add_fusion), dimensions={0} | reverse | bytes 2097152 | tf_op jit(solution)/shard_map/jit(_flip)/rev | solution.py:157
  141.8 9.5 %rev.18 = f32[1024,2,128]{0,2,1:T(8,128)} reverse(f32[1024,2,128]{0,2,1:T(8,128)} %bitcast.605), dimensions={0} | reverse | bytes 2097152 | tf_op jit(solution)/shard_map/jit(_flip)/rev | solution.py:155
  158.6 7.5 %reverse.3 = f32[1024,2,128]{0,2,1:T(8,128)S(1)} reverse(f32[1024,2,128]{0,2,1:T(8,128)} %bitcast.591), dimensions={0} | reverse | bytes 2097152 | tf_op jit(solution)/shard_map/reverse
  172.9 8.7 %rev.19 = bf16[1024,2,128]{0,2,1:T(8,128)(2,1)} reverse(bf16[1024,2,128]{0,2,1:T(8,128)(2,1)} %bitcast.608), dimensions={0} | reverse | bytes 1048576 | tf_op jit(solution)/shard_map/jit(_flip)/rev | solution.py:156
  183.8 4.1 exponential_multiply_fusion
  190.1 13.5 %while.27 = (s32[]{:T(128)}, f32[2,128,128]{2,1,0:T(8,128)S(1)}, bf16[8,2,128,128]{3,2,1,0:T(8,128)(2,1)}, f32[8,2,128]{2,0,1:T(8,128)S(1)}, f32[8,2,128,128]{3,2,1,0:T(8,128)}, /*index=5*/s32[]{:T(128)}, s32[]{:T(128)}) while((s32[]{:T(128)}, f32[2,128,128]{2,1,0:T(8,128)S(1)}, bf16[8,2,128,128]{3,2,1,0:T(8,128)(2,1)}, ...), condition=%wide.region_7.8_spmd.clone, body=%wide.region_6.7_spmd.clone.sunk | while | flops 131075 | bytes 593504 | solution.py:109
  203.6 8.9 %all-gather.5 = bf16[2,2,128]{2,1,0:T(2,128)(2,1)S(1)} all-gather(bf16[1,2,128]{2,1,0:T(2,128)(2,1)S(1)} %fusion.229), channel_id=4, replica_groups=mesh['grp'=2,'ep_0'=16,'ep_1'=2,'tp'=4] {'ep_1'}, dimensions={0}, use_global_device_ids=true | all-gather | bytes 1536 | tf_op jit(solution)/shard_map/all_gather | solution.py:31
  242.4 13.5 %while.26 = (s32[]{:T(128)}, f32[2,128,128]{2,1,0:T(8,128)S(1)}, bf16[8,2,128,128]{3,2,1,0:T(8,128)(2,1)}, f32[8,2,128]{2,0,1:T(8,128)S(1)}, f32[8,2,128,128]{3,2,1,0:T(8,128)}, /*index=5*/s32[]{:T(128)}, s32[]{:T(128)}) while((s32[]{:T(128)}, f32[2,128,128]{2,1,0:T(8,128)S(1)}, bf16[8,2,128,128]{3,2,1,0:T(8,128)(2,1)}, ...), condition=%wide.region_2.3_spmd.clone, body=%wide.region_1.2_spmd.clone.sunk | while | flops 131075 | bytes 593504 | solution.py:109
  282.6 8.5 %convolution_minimum_fusion = f32[1536,512]{1,0:T(8,128)} fusion(bf16[1536,2048]{1,0:T(8,128)(2,1)} %all-gather.14.cloned.1.call-done, bf16[1,2048,512]{2,1,0:T(8,128)(2,1)} %param.29), kind=kOutput, calls=%fused_computation.12 | convolution fusion | flops 3222011904 | bytes 11534336 | tf_op jit(solution)/shard_map/dot_general | solution.py:211
  291.1 11.9 %convolution_convert_fusion = bf16[1536,2048]{1,0:T(8,128)(2,1)} fusion(bf16[1,512,2048]{2,1,0:T(8,128)(2,1)S(1)} %copy-done, f32[1536,512]{1,0:T(8,128)} %convolution_minimum_fusion, bf16[1536,2048]{1,0:T(8,128)(2,1)} %all-gather.14.cloned.1.call-done, bf16[1,2048,512]{2,1,0:T(8,128)(2,1)} %param.30), kind=kOutput, calls=%fused_computation.9 | convolution fusion | flops 6452674560 | bytes 19922944 | tf_op jit(solution)/shard_map/dot_general | solution.py:225
  303.0 5.5 %all-to-all-start.2 = ((bf16[4,384,2048]{2,1,0:T(8,128)(2,1)}), bf16[4,384,2048]{2,1,0:T(8,128)(2,1)}, u32[]{:S(2)}, u32[]{:S(2)}) async-start(bf16[4,384,2048]{2,1,0:T(8,128)(2,1)} %bitcast.593), calls=%async_computation.3 | async-start | bytes 12582912 | tf_op jit(solution)/shard_map/all_to_all | solution.py:74
  310.3 26.4 %all_gather.45 = bf16[16,2,128]{2,1,0:T(2,128)(2,1)S(1)} all-gather(bf16[1,2,128]{2,1,0:T(2,128)(2,1)S(1)} %copy-done.32), channel_id=1, replica_groups=mesh['grp'=2,'ep_0'=16,'ep_1'=2,'tp'=4] {'ep_0'}, dimensions={0}, use_global_device_ids=true | all-gather | bytes 8704 | tf_op jit(solution)/shard_map/all_gather | solution.py:31
  336.7 22.5 %all_gather.40 = bf16[16,2,128]{2,1,0:T(2,128)(2,1)S(1)} all-gather(bf16[1,2,128]{2,1,0:T(2,128)(2,1)S(1)} %copy-done.33), channel_id=1, replica_groups=mesh['grp'=2,'ep_0'=16,'ep_1'=2,'tp'=4] {'ep_0'}, dimensions={0}, use_global_device_ids=true | all-gather | bytes 8704 | tf_op jit(solution)/shard_map/all_gather | solution.py:31
  360.5 3.9 fusion.7
  364.4 7.5 %rev.20 = f32[1024,2,128]{0,2,1:T(8,128)S(1)} reverse(f32[1024,2,128]{0,2,1:T(8,128)} %fusion.7), dimensions={0} | reverse | bytes 2097152 | tf_op jit(solution)/shard_map/jit(_flip)/rev | solution.py:160
  379.5 4.2 reduce_sum.74
  385.3 13.2 %all-to-all-start.3 = ((bf16[32,12,2048]{2,1,0:T(8,128)(2,1)}), bf16[32,12,2048]{2,1,0:T(8,128)(2,1)S(1)}, u32[]{:S(2)}, u32[]{:S(2)}) async-start(bf16[32,12,2048]{2,1,0:T(8,128)(2,1)} %all_to_all.20), calls=%async_computation.4 | async-start | bytes 4194304 | tf_op jit(solution)/shard_map/all_to_all | solution.py:229
  398.6 98.0 %all-to-all-done.3 = bf16[32,12,2048]{2,1,0:T(8,128)(2,1)S(1)} async-done(((bf16[32,12,2048]{2,1,0:T(8,128)(2,1)}), bf16[32,12,2048]{2,1,0:T(8,128)(2,1)S(1)}, u32[]{:S(2)}, u32[]{:S(2)}) %all-to-all-start.3) | async-done | bytes 1572896 | tf_op jit(solution)/shard_map/all_to_all | solution.py:229
  498.0 4.1 gather_fusion.1
  504.4 5.6 %multiply_reduce_fusion = bf16[128,2048]{1,0:T(8,128)(2,1)} fusion(f32[128,2,2048]{2,1,0:T(2,128)} %reshape.607, f32[128,2]{1,0:T(8,128)S(1)} %copy.153), kind=kLoop, calls=%fused_computation.20 | loop fusion | flops 786432 | bytes 2622464 | tf_op jit(solution)/shard_map/reduce_sum | solution.py:231
  (240 shorter events, 141.3 us)
Async XLA Ops:
  7.2 283.9 %copy-start = (bf16[1,512,2048]{2,1,0:T(8,128)(2,1)S(1)}, bf16[1,512,2048]{2,1,0:T(8,128)(2,1)}, u32[]{:S(2)}) copy-start(bf16[1,512,2048]{2,1,0:T(8,128)(2,1)} %param.31) | copy-start | bytes 6291460
  7.2 275.4 %all-gather.14.cloned.1.call-start = ((), (), s32[]{:S(2)}) async-start(), calls=%async_computation.8 | async-start | bytes 7864320 | tf_op jit(solution)/shard_map/all_gather | solution.py:210
  128.0 232.3 %all-gather.12.cloned.1.call-start = ((), (), s32[]{:S(2)}) async-start(), calls=%async_computation.6 | async-start | bytes 1114112 | tf_op jit(solution)/shard_map/all_gather | solution.py:31
  141.8 16.8 %copy-start.2 = (f32[8,128,2,128]{3,0,1,2:T(8,128)}, f32[8,128,2,128]{3,0,1,2:T(8,128)S(1)}, u32[]{:S(2)}) copy-start(f32[8,128,2,128]{3,0,1,2:T(8,128)S(1)} %fusion.22) | copy-start | bytes 3145732
  168.2 15.5 %slice-start = ((f32[8,128,2,128]{3,0,1,2:T(8,128)}), f32[8,1,2,128]{3,0,1,2:T(8,128)S(1)}, s32[]{:S(2)}) async-start(f32[8,128,2,128]{3,0,1,2:T(8,128)} %copy-done.2), calls=%async_computation.9 | async-start | bytes 16384 | tf_op jit(solution)/shard_map/slice | solution.py:95
  168.2 15.5 %copy-start.3 = (f32[8,128,2,128]{3,0,1,2:T(8,128)S(1)}, f32[8,128,2,128]{3,0,1,2:T(8,128)}, u32[]{:S(2)}) copy-start(f32[8,128,2,128]{3,0,1,2:T(8,128)} %copy-done.2) | copy-start | bytes 3145732
  215.0 9.5 %copy-start.24 = (f32[2,128]{1,0:T(2,128)}, f32[2,128]{1,0:T(2,128)S(1)}, u32[]{:S(2)}) copy-start(f32[2,128]{1,0:T(2,128)S(1)} %fusion.245) | copy-start | bytes 3076
  215.9 156.0 %all-gather.10.cloned.1.call-start = ((), (), s32[]{:S(2)}) async-start(), calls=%async_computation.5 | async-start | bytes 1114112 | tf_op jit(solution)/shard_map/all_gather | solution.py:31
  303.0 76.5 %all-to-all-start.2 = ((bf16[4,384,2048]{2,1,0:T(8,128)(2,1)}), bf16[4,384,2048]{2,1,0:T(8,128)(2,1)}, u32[]{:S(2)}, u32[]{:S(2)}) async-start(bf16[4,384,2048]{2,1,0:T(8,128)(2,1)} %bitcast.593), calls=%async_computation.3 | async-start | bytes 12582912 | tf_op jit(solution)/shard_map/all_to_all | solution.py:74
  308.5 201.5 %reduce-scatter.2.cloned.1.call-start = ((), (), s32[]{:S(2)}) async-start(), calls=%async_computation.7 | async-start | bytes 5242880 | tf_op jit(solution)/shard_map/reduce_scatter | solution.py:215
  308.6 28.1 %copy-start.33 = (bf16[1,2,128]{2,1,0:T(2,128)(2,1)S(1)}, bf16[1,2,128]{2,1,0:T(2,128)(2,1)}, u32[]{:S(2)}) copy-start(bf16[1,2,128]{2,1,0:T(2,128)(2,1)} %get-tuple-element.210) | copy-start | bytes 1540
  308.6 51.8 %copy-start.7 = (f32[1024,2,128]{0,2,1:T(8,128)S(1)}, f32[1024,2,128]{0,2,1:T(8,128)}, u32[]{:S(2)}) copy-start(f32[1024,2,128]{0,2,1:T(8,128)} %copy-done.6) | copy-start | bytes 3145732
  308.6 51.8 %copy-start.13 = (f32[1024,2,128]{0,2,1:T(8,128)S(1)}, f32[1024,2,128]{0,2,1:T(8,128)}, u32[]{:S(2)}) copy-start(f32[1024,2,128]{0,2,1:T(8,128)} %reshape.532) | copy-start | bytes 3145732
  308.6 51.8 %copy-start.21 = (f32[2,128]{1,0:T(2,128)S(1)}, f32[2,128]{1,0:T(2,128)}, u32[]{:S(2)}) copy-start(f32[2,128]{1,0:T(2,128)} %copy-done.20) | copy-start | bytes 3076
  308.6 51.8 %copy-start.25 = (f32[2,128]{1,0:T(2,128)S(1)}, f32[2,128]{1,0:T(2,128)}, u32[]{:S(2)}) copy-start(f32[2,128]{1,0:T(2,128)} %copy-done.24) | copy-start | bytes 3076
  308.6 51.8 %copy-start.28 = (f32[2,128]{1,0:T(2,128)S(1)}, f32[2,128]{1,0:T(2,128)}, u32[]{:S(2)}) copy-start(f32[2,128]{1,0:T(2,128)} %get-tuple-element.215) | copy-start | bytes 3076
  360.4 11.5 %copy-start.8 = (f32[1024,256]{0,1:T(8,128)S(1)}, f32[1024,256]{0,1:T(8,128)}, u32[]{:S(2)}) copy-start(f32[1024,256]{0,1:T(8,128)} %get-tuple-element.175) | copy-start | bytes 3145732
  360.4 11.5 %copy-start.23 = (f32[2,128]{1,0:T(2,128)S(1)}, f32[2,128]{1,0:T(2,128)}, u32[]{:S(2)}) copy-start(f32[2,128]{1,0:T(2,128)} %copy-done.22) | copy-start | bytes 3076
  360.5 11.5 %copy-start.27 = (f32[2,128]{1,0:T(2,128)S(1)}, f32[2,128]{1,0:T(2,128)}, u32[]{:S(2)}) copy-start(f32[2,128]{1,0:T(2,128)} %copy-done.26) | copy-start | bytes 3076
  360.5 11.5 %copy-start.29 = (f32[2,128]{1,0:T(2,128)S(1)}, f32[2,128]{1,0:T(2,128)}, u32[]{:S(2)}) copy-start(f32[2,128]{1,0:T(2,128)} %get-tuple-element.212) | copy-start | bytes 3076
  383.7 14.7 %copy-start.35 = (f32[128,2]{0,1:T(2,128)S(1)}, f32[128,2]{0,1:T(2,128)}, u32[]{:S(2)}) copy-start(f32[128,2]{0,1:T(2,128)} %param.28) | copy-start | bytes 3076
  383.7 14.8 %copy-start.31 = (s32[256,1]{0,1:T(1,128)S(1)}, s32[256,1]{0,1:T(1,128)}, u32[]{:S(2)}) copy-start(s32[256,1]{0,1:T(1,128)} %copy-done.30) | copy-start | bytes 3076
  385.3 111.4 %all-to-all-start.3 = ((bf16[32,12,2048]{2,1,0:T(8,128)(2,1)}), bf16[32,12,2048]{2,1,0:T(8,128)(2,1)S(1)}, u32[]{:S(2)}, u32[]{:S(2)}) async-start(bf16[32,12,2048]{2,1,0:T(8,128)(2,1)} %all_to_all.20), calls=%async_computation.4 | async-start | bytes 4194304 | tf_op jit(solution)/shard_map/all_to_all | solution.py:229
  498.0 12.0 %copy-start.1 = (bf16[1,512,2048]{2,1,0:T(8,128)(2,1)S(1)}, bf16[1,512,2048]{2,1,0:T(8,128)(2,1)}, u32[]{:S(2)}) copy-start(bf16[1,512,2048]{2,1,0:T(8,128)(2,1)} %param.31) | copy-start | bytes 6291460
  (20 other events, 74.6 us)
Sparse Core Ops, SparseCore 0:
  128.1 74.5 all-gather.13
  216.0 54.1 all-gather.11
  272.0 67.5 all-gather.9
  378.8 55.3 reduce-scatter.1
where the time goes:
time: 527 us; the launch traced here: 517 us
  blocking collectives  161 us (31%)
  local copies, waits for them, and re-layouts  116 us (22%)
  waiting for transfers between devices  99.1 us (19%)
  other arithmetic  63 us (12%)
  matrix products  43.6 us (8%)
  starting transfers between devices  19.4 us (4%)
  between operations  14.8 us (3%)
    all_to_all x1, waiting for transfers between devices, body(): lax.all_to_all(expert_sum, EP, split_axis=0, concat_axis=0, tiled=True)  98 us
    all_to_all x2, blocking collectives, turned_blocks(): result = lax.all_to_all(result, axes[k], k, k, tiled=True)  97.1 us
    all_gather x6, blocking collectives, entering_2(): lax.all_gather(part.astype(kind), axis)  63.7 us
    add x16, other arithmetic, advance(): return (state * decay[..., None] + increment, state)  16.3 us
    unnamed x83, local copies, waits for them, and re-layouts  15.2 us
    all_to_all x1, starting transfers between devices, body(): lax.all_to_all(expert_sum, EP, split_axis=0, concat_axis=0, tiled=True)  13.2 us
    rev x2, local copies, waits for them, and re-layouts, mixer_head_states(): jnp.flip(ending_state, 0)  12 us
    dot_general x1, matrix products, body(): jnp.dot(picked, down_weight[0], preferred_element_type=jnp.float32)  11.9 us
  transfers between devices with their start and end apart: 6, of which 2 were waited for; matrix products, arithmetic and copies ran while one was open for 37% of the time, Pallas kernels for 0%

commit v1 on v0

v1 whole, which is shorter than its diff:
```python
import functools

import jax
import jax.numpy as jnp
import numpy as np
from jax import lax
from jax.experimental import pallas as pl
from jax.experimental.pallas import tpu as pltpu
from jax.sharding import PartitionSpec as P

F32, BF16 = jnp.float32, jnp.bfloat16
HC = 128
BLK = 128
CAP = 12
QUARTERS = 4
EPS = 1e-06
LIMIT = 7.0
SLOPE = 1.702
VMEM = pltpu.VMEM
MESH = pl.DeviceIdType.MESH
WHOLE = pl.BlockSpec(memory_space=VMEM)
ANYWHERE = pl.BlockSpec(memory_space=pl.ANY)


def mm(a, b):
    return jnp.dot(a, b, preferred_element_type=F32)


def mm_t(a, b):
    return lax.dot_general(a, b, (((1,), (1,)), ((), ())), preferred_element_type=F32)


def t_mm(a, b):
    return lax.dot_general(a, b, (((0,), (0,)), ((), ())), preferred_element_type=F32)


def iota(shape, dim):
    return lax.broadcasted_iota(jnp.int32, shape, dim)


def silu_sigmoid(x):
    return 1.0 / (1.0 + jnp.exp(-x))


def recurrence_states(
    q_ref, g_ref, v_ref, margin_ref, pos_ref, qin, kin, before, off, fin, inc, last
):
    blocks = q_ref.shape[0] // BLK
    heads = q_ref.shape[1] // HC
    row, col = iota((BLK, BLK), 0), iota((BLK, BLK), 1)
    tri = ((row >= col).astype(BF16), (row <= col).astype(BF16))
    ends = [jnp.exp(margin_ref[d : d + 1, :]) for d in range(2)]

    def per_block(n, carry):
        rows = pl.ds(pl.multiple_of(n * BLK, BLK), BLK)
        q = q_ref[rows, :].astype(F32)
        q = q * silu_sigmoid(q) * HC**-0.5
        shut = silu_sigmoid(-g_ref[rows, :].astype(F32))
        values = v_ref[rows, :]
        pos = pos_ref[rows, :]
        pos = jnp.concatenate(
            [jnp.broadcast_to(pos[:, h : h + 1], (BLK, HC)) for h in range(heads)], axis=1
        )
        for d in range(2):
            k = ends[d] * shut
            logs = jnp.log1p(-k) + pos
            high = logs.astype(BF16)
            low = (logs - high.astype(F32)).astype(BF16)
            cum = mm(tri[d], high) + mm(tri[d], low)
            end = cum[BLK - 1 :, :] if d == 0 else cum[:1, :]
            qin[d, rows, :] = (q * jnp.exp(cum)).astype(BF16)
            kin[d, rows, :] = (k * jnp.exp(-cum)).astype(BF16)
            ks = (k * jnp.exp(end - cum)).astype(BF16)
            last[d, n] = end
            for h in range(heads):
                cols = slice(h * HC, (h + 1) * HC)
                inc[d, n, h] = t_mm(values[:, cols], ks[:, cols])
        return carry

    lax.fori_loop(0, blocks, per_block, 0)
    slab = iota((16, HC), 0)
    for d in range(2):

        def chain(i, carry):
            n = i if d == 0 else blocks - 1 - i
            offset, states = carry
            off[d, n] = offset
            end = last[d, n]
            decay = jnp.exp(end)
            new = []
            for h in range(heads):
                before[d, n, h] = states[h]
                new.append(states[h] * decay[:, h * HC : (h + 1) * HC] + inc[d, n, h])
            return offset + end, tuple(new)

        zero = tuple(jnp.zeros((HC, HC), F32) for _ in range(heads))
        total, states = lax.fori_loop(0, blocks, chain, (jnp.zeros((1, heads * HC), F32), zero))
        decay = jnp.exp(total)
        for h in range(heads):
            fin[d * heads + h, :HC, :] = states[h].astype(BF16)
            part = decay[:, h * HC : (h + 1) * HC]
            high = part.astype(BF16).astype(F32)
            fin[d * heads + h, HC:, :] = jnp.where(
                slab == 0, high, jnp.where(slab == 1, part - high, 0.0)
            ).astype(BF16)


def recurrence_outputs(qin, kin, v_ref, before, off, every, me_ref, gain, out, entering):
    blocks = v_ref.shape[0] // BLK
    heads = v_ref.shape[1] // HC
    devices = every.shape[0]
    me = me_ref[0]
    for d in range(2):
        for h in range(heads):
            at = d * heads + h

            def combine(i, state):
                j = i if d == 0 else devices - 1 - i
                decay = jnp.sum(every[j, at, HC:, :].astype(F32), axis=0, keepdims=True)
                passed = (j < me) if d == 0 else (j > me)
                return jnp.where(passed, state * decay + every[j, at, :HC, :].astype(F32), state)

            entering[at] = lax.fori_loop(0, devices, combine, jnp.zeros((HC, HC), F32))
    row, col = iota((BLK, BLK), 0), iota((BLK, BLK), 1)

    def per_block(n, carry):
        rows = pl.ds(pl.multiple_of(n * BLK, BLK), BLK)
        for h in range(heads):
            cols = slice(h * HC, (h + 1) * HC)
            scores, outer = [], None
            for d in range(2):
                q = qin[d, rows, cols]
                scores.append(mm_t(q, kin[d, rows, cols]))
                state = before[d, n, h] + entering[d * heads + h] * jnp.exp(off[d, n, :, cols])
                part = mm_t(q, state.astype(BF16))
                outer = part if outer is None else outer + part
            both = jnp.where(row >= col, scores[0], 0.0) + jnp.where(row <= col, scores[1], 0.0)
            mix = mm(both.astype(BF16), v_ref[rows, cols]) + outer
            scale = lax.rsqrt(jnp.mean(mix * mix, axis=1, keepdims=True) + EPS)
            out[rows, cols] = (mix * scale * gain[...]).astype(BF16)
        return carry

    lax.fori_loop(0, blocks, per_block, 0)


def pack_rows(tok_ref, gain_ref, routes_ref, slot_ref, quarter_ref, send, *, experts):
    x = tok_ref[...].astype(F32)
    count, features = x.shape
    width = features // QUARTERS
    scale = lax.rsqrt(jnp.mean(x * x, axis=1, keepdims=True) + EPS)
    normed = (x * scale * gain_ref[...]).astype(BF16)
    routes = routes_ref[...]
    names = iota((experts, count), 0)
    hot = [(routes[k : k + 1, :] == names).astype(F32) for k in range(2)]
    earlier = (iota((count, count), 0) < iota((count, count), 1)).astype(BF16)
    rank = mm((hot[0] + hot[1]).astype(BF16), earlier)
    base = names.astype(F32) * CAP
    dest = [jnp.sum(hot[k] * (rank + base), axis=0, keepdims=True) for k in range(2)]
    slot = slot_ref[...]
    picked = jnp.logical_or(slot == dest[0], slot == dest[1])
    quarter = quarter_ref[...]
    lhs = jnp.concatenate(
        [jnp.where(jnp.logical_and(picked, quarter == q), 1.0, 0.0) for q in range(QUARTERS)],
        axis=1,
    ).astype(BF16)
    rhs = jnp.concatenate([normed[:, q * width : (q + 1) * width] for q in range(QUARTERS)], axis=0)
    send[...] = mm(lhs, rhs).astype(BF16)


def merge_rows(ret_ref, routes_ref, weight_ref, slot_ref, quarter_ref, out, *, experts):
    routes = routes_ref[...]
    count = routes.shape[0]
    names = iota((count, experts), 1)
    hot = [(routes[:, k : k + 1] == names).astype(F32) for k in range(2)]
    earlier = (iota((count, count), 0) > iota((count, count), 1)).astype(BF16)
    rank = mm(earlier, (hot[0] + hot[1]).astype(BF16))
    base = names.astype(F32) * CAP
    slot, quarter = slot_ref[...], quarter_ref[...]
    weight = weight_ref[...]
    rows = ret_ref[...]
    width = rows.shape[1]
    totals = [None] * QUARTERS
    for k in range(2):
        dest = jnp.sum(hot[k] * (rank + base), axis=1, keepdims=True)
        picked = slot == dest
        lhs = jnp.concatenate(
            [jnp.where(jnp.logical_and(picked, quarter == q), 1.0, 0.0) for q in range(QUARTERS)],
            axis=0,
        ).astype(BF16)
        got = mm(lhs, rows)
        for q in range(QUARTERS):
            part = weight[:, k : k + 1] * got[q * count : (q + 1) * count, :]
            totals[q] = part if k == 0 else totals[q] + part
    for q in range(QUARTERS):
        out[:, q * width : (q + 1) * width] = totals[q].astype(BF16)


def expert_kernel(
    send, wg_any, wu_any, wd_any, perm, perm_t, ret,
    rows, parts, relay_l, relay_r, from_l, from_r, total, xt, wg, wu, wd,
    w_sem, zs, zr, xs, xr_l, xr_r, ys, yr, qs, qr, fs, fr, ts, tr,
    *, n_ep, n_tp,
):
    me, t = lax.axis_index("ep"), lax.axis_index("tp")
    n_z = n_ep // 2
    half = n_z // 2
    steps = n_z // 2
    z, c = me // 2, me % 2
    right, left = (t + 1) % n_tp, (t + n_tp - 1) % n_tp
    chunk = send.shape[1]
    width = send.shape[2]

    def offset(b, side):
        o = (steps + 1 - b) % steps
        return o if side == 0 else n_z - o - half * ((steps - o) // steps)

    weights = [
        pltpu.make_async_copy(src.at[0], dst, w_sem.at[i])
        for i, (src, dst) in enumerate(((wg_any, wg), (wu_any, wu), (wd_any, wd)))
    ]
    for copy in weights:
        copy.start()

    barrier = pltpu.get_barrier_semaphore()

    def greet(j, carry):
        pl.semaphore_signal(
            barrier, inc=1, device_id={"ep": (me + j) % n_ep}, device_id_type=MESH
        )
        return carry

    lax.fori_loop(1, n_ep, greet, 0)
    for other in (left, right):
        pl.semaphore_signal(barrier, inc=1, device_id={"tp": other}, device_id_type=MESH)
    pl.semaphore_wait(barrier, n_ep + 1)

    def z_copy(b, side, core):
        other = ((z + offset(b, side)) % n_z) * 2 + core
        return pltpu.make_async_remote_copy(
            src_ref=send.at[other],
            dst_ref=rows.at[0, 4 * b + 2 * side + c],
            send_sem=zs.at[4 * b + 2 * side + core],
            recv_sem=zr.at[4 * b + 2 * side + c],
            device_id={"ep": other},
            device_id_type=MESH,
        )

    def own_in(slot):
        return pltpu.make_async_copy(send.at[me], rows.at[0, slot], zr.at[slot])

    def is_self(b, side, core):
        return jnp.logical_and(jnp.logical_and(b == 1, side == 0), core == c)

    def dispatch(b, carry):
        for side in range(2):
            for core in range(2):
                own = is_self(b, side, core)

                @pl.when(own)
                def _():
                    own_in(4 * b + 2 * side + c).start()

                @pl.when(jnp.logical_not(own))
                def _():
                    z_copy(b, side, core).start()

        return carry

    lax.fori_loop(0, steps, dispatch, 0)

    def x_copy(b, way):
        group = pl.ds(4 * b, 4)
        return pltpu.make_async_remote_copy(
            src_ref=rows.at[0, group],
            dst_ref=rows.at[1 + way, group],
            send_sem=xs.at[way, b],
            recv_sem=(xr_l if way == 0 else xr_r).at[b],
            device_id={"tp": right if way == 0 else left},
            device_id_type=MESH,
        )

    def y_copy(b, way):
        group = pl.ds(4 * b + 2 * way, 2)
        return pltpu.make_async_remote_copy(
            src_ref=rows.at[1 + way, group],
            dst_ref=rows.at[3, group],
            send_sem=ys.at[way, b],
            recv_sem=yr.at[way, b],
            device_id={"tp": right if way == 0 else left},
            device_id_type=MESH,
        )

    def q_copy(b, way):
        return pltpu.make_async_remote_copy(
            src_ref=parts.at[3, pl.ds(4 * b + 2 * way, 2)],
            dst_ref=(relay_l if way == 0 else relay_r).at[pl.ds(2 * b, 2)],
            send_sem=qs.at[way, b],
            recv_sem=qr.at[way, b],
            device_id={"tp": right if way == 0 else left},
            device_id_type=MESH,
        )

    def f_copy(b, way):
        group = pl.ds(4 * b, 4)
        return pltpu.make_async_remote_copy(
            src_ref=parts.at[2 - way, group],
            dst_ref=(from_l if way == 0 else from_r).at[group],
            send_sem=fs.at[way, b],
            recv_sem=fr.at[way, b],
            device_id={"tp": right if way == 0 else left},
            device_id_type=MESH,
        )

    def t_copy(b, side, core):
        other = ((z - offset(b, side) + n_z) % n_z) * 2 + core
        slot = 4 * b + 2 * side + core
        return pltpu.make_async_remote_copy(
            src_ref=total.at[slot],
            dst_ref=ret.at[me],
            send_sem=ts.at[slot],
            recv_sem=tr.at[me],
            device_id={"ep": other},
            device_id_type=MESH,
        )

    def t_arrival(e):
        return pltpu.make_async_copy(total.at[0], ret.at[e], tr.at[e])

    def own_out(slot):
        return pltpu.make_async_copy(total.at[slot], ret.at[me], tr.at[me])

    def arrive(b):
        for k in range(4):
            own_in(4 * b + k).wait()
        x_copy(b, 0).start()
        x_copy(b, 1).start()

    def relay(b):
        for way in range(2):
            x_copy(b, way).wait_recv()
            y_copy(b, way).start()

    def compute(b):
        group = pl.ds(4 * b, 4)
        for way in range(2):
            y_copy(b, way).wait_recv()
        side = perm[...]
        for w in range(4):
            turned = mm(side, rows[w, group].reshape(4 * chunk, width)).astype(BF16)
            for q in range(QUARTERS):
                xt[w * chunk : (w + 1) * chunk, q * width : (q + 1) * width] = turned[
                    q * chunk : (q + 1) * chunk
                ]
        x = xt[...]
        gate = jnp.minimum(mm(x, wg[...]), LIMIT)
        up = jnp.clip(mm(x, wu[...]), -LIMIT, LIMIT)
        hidden = ((up + 1.0) * gate / (1.0 + jnp.exp(-SLOPE * gate))).astype(BF16)
        y = mm(hidden, wd[...]).astype(BF16)
        back = perm_t[...]
        for w in range(4):
            piece = jnp.concatenate(
                [
                    y[w * chunk : (w + 1) * chunk, q * width : (q + 1) * width]
                    for q in range(QUARTERS)
                ],
                axis=0,
            )
            parts[w, group] = mm(back, piece).astype(BF16).reshape(4, chunk, width)

    def start_sum(b):
        for way in range(2):
            q_copy(b, way).start()

    def pass_sum(b):
        for way in range(2):
            q_copy(b, way).wait_recv()
            group = pl.ds(4 * b + 2 * way, 2)
            carried = (relay_l if way == 0 else relay_r)[pl.ds(2 * b, 2)]
            parts[2 - way, group] = (
                parts[2 - way, group].astype(F32) + carried.astype(F32)
            ).astype(BF16)

    def send_sum(b):
        for way in range(2):
            f_copy(b, way).start()

    def finish(b):
        for way in range(2):
            f_copy(b, way).wait_recv()
        group = pl.ds(4 * b, 4)
        total[group] = (
            parts[0, group].astype(F32) + from_l[group].astype(F32) + from_r[group].astype(F32)
        ).astype(BF16)

    def send_back(b):
        for side in range(2):
            for core in range(2):
                own = is_self(b, side, core)

                @pl.when(own)
                def _():
                    own_out(4 * b + 2 * side + core).start()

                @pl.when(jnp.logical_not(own))
                def _():
                    t_copy(b, side, core).start()

    for copy in weights:
        copy.wait()

    def body(i, carry):
        def stage(lag, fn):
            @pl.when(jnp.logical_and(i >= lag, i < steps + lag))
            def _():
                fn(i - lag)

        stage(4, finish)
        stage(3, pass_sum)
        stage(2, compute)
        stage(4, send_back)
        stage(3, send_sum)
        stage(1, relay)
        stage(2, start_sum)
        stage(0, arrive)
        return carry

    lax.fori_loop(0, steps + 4, body, 0)

    def sent(b, carry):
        for way in range(2):
            x_copy(b, way).wait_send()
            y_copy(b, way).wait_send()
            q_copy(b, way).wait_send()
            f_copy(b, way).wait_send()
        for side in range(2):
            for core in range(2):

                @pl.when(jnp.logical_not(is_self(b, side, core)))
                def _():
                    z_copy(b, side, core).wait_send()
                    t_copy(b, side, core).wait_send()

        return carry

    lax.fori_loop(0, steps, sent, 0)

    def returned(e, carry):
        t_arrival(e).wait()
        return carry

    lax.fori_loop(0, n_ep, returned, 0)


def run_experts(send, wg, wu, wd, n_ep, n_tp):
    chunk, width = send.shape[1:]
    group = 4 * chunk
    ff, features = wd.shape[1:]
    source = np.arange(group)
    target = (source % chunk) // CAP * chunk + source // chunk * CAP + source % CAP
    perm = np.zeros((group, group), np.float32)
    perm[target, source] = 1.0
    many = send.shape
    steps = n_ep // 4
    dma = pltpu.SemaphoreType.DMA
    return pl.pallas_call(
        functools.partial(expert_kernel, n_ep=n_ep, n_tp=n_tp),
        out_shape=jax.ShapeDtypeStruct(many, BF16),
        in_specs=[WHOLE, ANYWHERE, ANYWHERE, ANYWHERE, WHOLE, WHOLE],
        out_specs=WHOLE,
        scratch_shapes=[
            VMEM((4, *many), BF16),
            VMEM((4, *many), BF16),
            VMEM((n_ep // 2, chunk, width), BF16),
            VMEM((n_ep // 2, chunk, width), BF16),
            VMEM(many, BF16),
            VMEM(many, BF16),
            VMEM(many, BF16),
            VMEM((group, features), BF16),
            VMEM(wg.shape[1:], BF16),
            VMEM(wu.shape[1:], BF16),
            VMEM(wd.shape[1:], BF16),
            dma((3,)),
            dma((n_ep,)), dma((n_ep,)),
            dma((2, steps)), dma((steps,)), dma((steps,)),
            dma((2, steps)), dma((2, steps)),
            dma((2, steps)), dma((2, steps)),
            dma((2, steps)), dma((2, steps)),
            dma((n_ep,)), dma((n_ep,)),
        ],
        compiler_params=pltpu.CompilerParams(
            collective_id=0, has_side_effects=True, vmem_limit_bytes=56 * 2**20
        ),
        cost_estimate=pl.CostEstimate(
            flops=60_000_000_000, bytes_accessed=10_000_000, transcendentals=0
        ),
        name="experts",
    )(send, wg, wu, wd, jnp.asarray(perm, BF16), jnp.asarray(perm.T, BF16))


def body(
    query, gates, value, margin, position, head_gain, mixer_weight,
    tokens, expert_gain, routes, weights, wg, wu, wd,
):
    n_ep, n_tp = lax.axis_size("ep"), lax.axis_size("tp")
    length, channels = query.shape
    heads, blocks = channels // HC, length // BLK
    count, features = tokens.shape

    states = jax.ShapeDtypeStruct((2, blocks, heads, HC, HC), F32)
    lines = jax.ShapeDtypeStruct((2, blocks, 1, channels), F32)
    streams = jax.ShapeDtypeStruct((2, length, channels), BF16)
    qin, kin, before, off, fin = pl.pallas_call(
        recurrence_states,
        out_shape=(
            streams, streams, states, lines,
            jax.ShapeDtypeStruct((2 * heads, HC + 16, HC), BF16),
        ),
        in_specs=[WHOLE] * 5,
        out_specs=[WHOLE] * 5,
        scratch_shapes=[VMEM(states.shape, F32), VMEM(lines.shape, F32)],
        compiler_params=pltpu.CompilerParams(vmem_limit_bytes=40 * 2**20),
        cost_estimate=pl.CostEstimate(
            flops=2_000_000_000, bytes_accessed=8_000_000, transcendentals=3_000_000
        ),
        name="states",
    )(query, gates, value, margin, jnp.transpose(position))
    every = lax.all_gather(fin, "ep")
    all_weight = lax.all_gather(mixer_weight, "tp")

    chunk = CAP * QUARTERS
    width = features // QUARTERS
    r = np.arange(n_ep * chunk)
    slot = (r // chunk * CAP + r % CAP).astype(np.float32)
    quarter = (r % chunk // CAP).astype(np.int32)
    send = pl.pallas_call(
        functools.partial(pack_rows, experts=n_ep),
        out_shape=jax.ShapeDtypeStruct((n_ep * chunk, width), BF16),
        in_specs=[WHOLE] * 5,
        out_specs=WHOLE,
        compiler_params=pltpu.CompilerParams(vmem_limit_bytes=40 * 2**20),
        name="pack",
    )(
        tokens, expert_gain[None, :], jnp.transpose(routes),
        jnp.asarray(slot[:, None]), jnp.asarray(quarter[:, None]),
    )
    ret = run_experts(send.reshape(n_ep, chunk, width), wg, wu, wd, n_ep, n_tp)
    ret, every, all_weight = lax.optimization_barrier((ret, every, all_weight))
    moe_out = pl.pallas_call(
        functools.partial(merge_rows, experts=n_ep),
        out_shape=jax.ShapeDtypeStruct((count, features), BF16),
        in_specs=[WHOLE] * 5,
        out_specs=WHOLE,
        compiler_params=pltpu.CompilerParams(vmem_limit_bytes=40 * 2**20),
        name="merge",
    )(
        ret.reshape(n_ep * chunk, width), routes, weights,
        jnp.asarray(slot[None, :]), jnp.asarray(quarter[None, :]),
    )

    heads_out = pl.pallas_call(
        recurrence_outputs,
        out_shape=jax.ShapeDtypeStruct((length, channels), BF16),
        in_specs=[WHOLE] * 6 + [pl.BlockSpec(memory_space=pltpu.SMEM), WHOLE],
        out_specs=WHOLE,
        scratch_shapes=[VMEM((2 * heads, HC, HC), F32)],
        compiler_params=pltpu.CompilerParams(vmem_limit_bytes=40 * 2**20),
        cost_estimate=pl.CostEstimate(
            flops=2_000_000_000, bytes_accessed=12_000_000, transcendentals=100_000
        ),
        name="outputs",
    )(qin, kin, value, before, off, every, lax.axis_index("ep")[None], head_gain[None, :])
    mine = lax.all_to_all(
        heads_out.reshape(n_tp, length // n_tp, channels), "tp", 0, 0, tiled=True
    )
    mixed = jnp.zeros((length // n_tp, features), F32)
    for g in range(n_tp):
        mixed = mixed + mm(mine[g], all_weight[g]).astype(BF16).astype(F32)
    return mixed.astype(BF16), moe_out


def solution(mesh):
    rows = P(("grp", "ep"), "tp")
    split = P(("grp", "ep", "tp"), None)
    return jax.shard_map(
        body,
        mesh=mesh,
        in_specs=(
            rows, rows, rows, P(None, "tp"), P("tp", ("grp", "ep")), P(), P("tp", None),
            split, P(), split, split,
            P("ep", None, "tp"), P("ep", None, "tp"), P("ep", "tp", None),
        ),
        out_specs=(split, split),
        check_vma=False,
    )
```

time: 527 us -> 260 us (0.49); the launches traced: 517 us -> 259 us
  Pallas kernels: 0 us -> 206 us
  blocking collectives: 161 us -> 0 us
  local copies, waits for them, and re-layouts: 116 us -> 18.2 us
  waiting for transfers between devices: 99.1 us -> 10.6 us
  other arithmetic: 63 us -> 0 us
  matrix products: 43.6 us -> 5.41 us
  starting transfers between devices: 19.4 us -> 4.15 us
    pallas_call x0 -> x5, Pallas kernels: none -> 206 us  [the longest x1 188 us: run_experts(): pl.pallas_call(functools.partial(expert_kernel, n_ep=n_ep, n_tp=n_tp), ou...]
    all_to_all x2 -> x0, blocking collectives: 97.1 us -> none  [turned_blocks(): result = lax.all_to_all(result, axes[k], k, k, tiled=True)]
    all_to_all x2 -> x1, waiting for transfers between devices: 98.9 us -> 4.46 us  [body(): lax.all_to_all(heads_out.reshape(n_tp, length // n_tp, channels), 'tp', 0...]
    all_gather x6 -> x0, blocking collectives: 63.7 us -> none  [entering_2(): lax.all_gather(part.astype(kind), axis)]
    rev x8 -> x0, local copies, waits for them, and re-layouts: 41.5 us -> none  [the longest x2 12 us: mixer_head_states(): jnp.flip(ending_state, 0)]
    dot_general x11 -> x4, matrix products: 43.6 us -> 5.41 us  [mm(): return jnp.dot(a, b, preferred_element_type=F32)]
    another operation x9 -> x0, local copies, waits for them, and re-layouts: 23.6 us -> none
    add x17 -> x0, other arithmetic: 16.4 us -> none  [the longest x16 16.3 us: advance(): return (state * decay[..., None] + increment, state)]
  transfers between devices with their start and end apart: 6 -> 3, of which waited for: 2 -> 2; matrix products, arithmetic and copies ran while one was open for 37% -> 1% of each run, Pallas kernels for 0% -> 77%
where the time goes in v1:
time: 260 us; the launch traced here: 259 us
  Pallas kernels  206 us (79%)
  local copies, waits for them, and re-layouts  18.2 us (7%)
  between operations  14.2 us (5%)
  waiting for transfers between devices  10.6 us (4%)
  matrix products  5.41 us (2%)
  starting transfers between devices  4.15 us (2%)
    pallas_call x1, Pallas kernels, run_experts(): pl.pallas_call(functools.partial(expert_kernel, n_ep=n_ep, n_tp=n_tp), ou...  188 us
    unnamed x45, local copies, waits for them, and re-layouts  18.2 us
    pallas_call x1, Pallas kernels, body(): pl.pallas_call(recurrence_states, out_shape=(streams, streams, states, li...  7.37 us
    pallas_call x1, Pallas kernels, body(): pl.pallas_call(recurrence_outputs, out_shape=jax.ShapeDtypeStruct((length...  6.67 us
    dot_general x4, matrix products, mm(): return jnp.dot(a, b, preferred_element_type=F32)  5.41 us
    all_gather x1, waiting for transfers between devices, body(): every = lax.all_gather(fin, 'ep')  5.36 us
  transfers between devices with their start and end apart: 3, of which 2 were waited for; matrix products, arithmetic and copies ran while one was open for 1% of the time, Pallas kernels for 77%

profile of v1, /device:TPU:33, one launch (start us, length us, event | category | flops | bytes accessed | tf_op | source)
XLA Modules:
  0.0 259.0 jit_solution(12039003884616415329)
XLA Ops:
  8.0 1.7 copy.25
  9.8 1.0 copy-done.7
  10.8 1.0 copy-done.9
  11.8 1.0 copy-done.16
  12.9 1.0 copy-done.17
  14.6 7.4 %states.1 = (bf16[2,1024,256]{2,1,0:T(8,128)(2,1)S(1)}, bf16[2,1024,256]{2,1,0:T(8,128)(2,1)S(1)}, f32[2,8,2,128,128]{4,3,2,1,0:T(8,128)S(1)}, f32[2,8,1,256]{3,2,1,0:T(1,128)S(1)}, bf16[4,144,128]{2,1,0:T(8,128)(2,1)}) custom-call(bf16[1024,256]{1,0:T(8,128)(2,1)S(1)} %copy-done.16, bf16[1024,256]{1,0:T(8,128)(2,1)S(1)} %copy-done.17, ...), custom_call_target="tpu_custom_call" | custom-call | flops 2000000000 | bytes 8000000 | tf_op jit(solution)/shard_map/states/pallas_call | solution.py:512
  23.1 1.1 copy-done.5
  24.2 1.1 copy-done.6
  25.3 1.0 copy-done.10
  26.4 1.6 pack.1
  28.0 1.1 copy-done.2
  29.1 187.9 %experts.1 = bf16[32,48,512]{2,1,0:T(8,128)(2,1)} custom-call(bf16[32,48,512]{2,1,0:T(8,128)(2,1)} %bitcast.36, bf16[1,2048,512]{2,1,0:T(8,128)(2,1)} %wg_any.1, bf16[1,2048,512]{2,1,0:T(8,128)(2,1)} %wu_any.1, bf16[1,512,2048]{2,1,0:T(8,128)(2,1)} %wd_any.1, bf16[192,192]{1,0:T(8,128)(2,1)} %constant.18.clone.perm.perm_t, ...), custom_call_target="tpu_custom_call" | custom-call | flops 60000002048 | bytes 10000000 | tf_op jit(solution)/shard_map/experts/pallas_call | solution.py:465
  217.0 5.4 %all-gather.5.cloned.1.call-done = bf16[128,144,128]{2,1,0:T(8,128)(2,1)} async-done(((bf16[4,144,128]{2,1,0:T(8,128)(2,1)}), bf16[128,144,128]{2,1,0:T(8,128)(2,1)}) %all-gather.5.cloned.1.call-update) | async-done | bytes 4718608 | tf_op jit(solution)/shard_map/all_gather | solution.py:527
  222.4 2.3 copy-done
  224.7 1.2 copy-done.4
  225.9 1.0 copy-done.8
  227.0 6.7 %outputs.1 = bf16[1024,256]{1,0:T(8,128)(2,1)} custom-call(bf16[2,1024,256]{2,1,0:T(8,128)(2,1)S(1)} %get-tuple-element.10.qin, bf16[2,1024,256]{2,1,0:T(8,128)(2,1)S(1)} %copy-done.4, bf16[1024,256]{1,0:T(8,128)(2,1)S(1)} %copy-done.8, f32[2,8,2,128,128]{4,3,2,1,0:T(8,128)S(1)} %get-tuple-element.12.before, f32[2,8,1,256]{3,2,1,0:T(1,128)S(1)} %get-tuple-element.13.off, ...), custom_call_target="tpu_custom_call" | custom-call | flops 2000000000 | bytes 12000000 | tf_op jit(solution)/shard_map/outputs/pallas_call | solution.py:560
  233.6 4.0 %all-to-all-start = ((bf16[4,256,256]{2,1,0:T(8,128)(2,1)}), bf16[4,256,256]{2,1,0:T(8,128)(2,1)S(1)}, u32[]{:S(2)}, u32[]{:S(2)}) async-start(bf16[4,256,256]{2,1,0:T(8,128)(2,1)} %bitcast.8), calls=%async_computation | async-start | bytes 1048576 | tf_op jit(solution)/shard_map/all_to_all | solution.py:572
  237.9 1.4 copy-done.1
  239.3 2.9 %merge.1 = bf16[128,2048]{1,0:T(8,128)(2,1)} custom-call(bf16[1536,512]{1,0:T(8,128)(2,1)S(1)} %bitcast.35, s32[128,2]{1,0:T(8,128)S(1)} %copy.26.routes_ref, f32[128,2]{1,0:T(8,128)S(1)} %copy.27.weight_ref, f32[1,1536]{1,0:T(1,128)S(1)} %copy-done.12, s32[1,1536]{1,0:T(1,128)S(1)} %copy-done.13), custom_call_target="tpu_custom_call" | custom-call | tf_op jit(solution)/shard_map/merge/pallas_call | solution.py:548
  242.2 4.5 %all-to-all-done = bf16[4,256,256]{2,1,0:T(8,128)(2,1)S(1)} async-done(((bf16[4,256,256]{2,1,0:T(8,128)(2,1)}), bf16[4,256,256]{2,1,0:T(8,128)(2,1)S(1)}, u32[]{:S(2)}, u32[]{:S(2)}) %all-to-all-start) | async-done | bytes 524320 | tf_op jit(solution)/shard_map/all_to_all | solution.py:572
  246.7 1.8 fusion.5
  248.5 1.7 fusion.6
  250.6 1.5 fusion.4
  (38 shorter events, 3.3 us)
Async XLA Ops:
  7.2 209.8 %all-gather.7.cloned.1.call-start = ((), (), s32[]{:S(2)}) async-start(), calls=%async_computation.2 | async-start | bytes 5242880 | tf_op jit(solution)/shard_map/all_gather | solution.py:528
  8.0 214.4 %all-gather.5.cloned.1.call-start = ((), (), s32[]{:S(2)}) async-start(), calls=%async_computation.1 | async-start | bytes 4866048 | tf_op jit(solution)/shard_map/all_gather | solution.py:527
  9.8 1.0 copy-start.7
  10.8 1.0 copy-start.9
  11.8 1.0 copy-start.16
  12.9 1.0 copy-start.17
  13.9 0.7 copy-start.18
  14.6 8.4 %copy-start.11 = (f32[2048]{0:T(1024)S(1)}, f32[2048]{0:T(1024)}, u32[]{:S(2)}) copy-start(f32[2048]{0:T(1024)} %param.28) | copy-start | bytes 24580
  14.6 8.4 %copy-start.14 = (s32[128,2]{0,1:T(2,128)S(1)}, s32[128,2]{0,1:T(2,128)}, u32[]{:S(2)}) copy-start(s32[128,2]{0,1:T(2,128)} %param.29) | copy-start | bytes 3076
  22.0 1.0 copy-start.3
  23.0 1.1 copy-start.5
  24.2 1.1 copy-start.6
  25.3 1.0 copy-start.10
  27.9 1.1 copy-start.2
  29.1 193.3 %copy-start.15 = (f32[128]{0:T(128)S(1)}, f32[128]{0:T(128)}, u32[]{:S(2)}) copy-start(f32[128]{0:T(128)} %param.25) | copy-start | bytes 1540
  222.3 2.3 copy-start
  224.7 1.2 copy-start.4
  225.9 1.0 copy-start.8
  227.0 10.8 %copy-start.20 = (f32[128,2]{0,1:T(2,128)S(1)}, f32[128,2]{0,1:T(2,128)}, u32[]{:S(2)}) copy-start(f32[128,2]{0,1:T(2,128)} %param.30) | copy-start | bytes 3076
  227.0 10.9 %copy-start.12 = (f32[1,1536]{1,0:T(1,128)S(1)}, f32[1,1536]{1,0:T(1,128)}, u32[]{:S(2)}) copy-start(f32[1,1536]{1,0:T(1,128)} %constant.19.clone.slot_ref) | copy-start | bytes 18436
  227.0 10.9 %copy-start.13 = (s32[1,1536]{1,0:T(1,128)S(1)}, s32[1,1536]{1,0:T(1,128)}, u32[]{:S(2)}) copy-start(s32[1,1536]{1,0:T(1,128)} %constant.20.clone.quarter_ref) | copy-start | bytes 18436
  233.6 13.0 %all-to-all-start = ((bf16[4,256,256]{2,1,0:T(8,128)(2,1)}), bf16[4,256,256]{2,1,0:T(8,128)(2,1)S(1)}, u32[]{:S(2)}, u32[]{:S(2)}) async-start(bf16[4,256,256]{2,1,0:T(8,128)(2,1)} %bitcast.8), calls=%async_computation | async-start | bytes 1048576 | tf_op jit(solution)/shard_map/all_to_all | solution.py:572
  237.9 1.4 copy-start.1
  246.7 3.5 %copy-start.19 = (bf16[1024,2048]{1,0:T(8,128)(2,1)S(1)}, bf16[1024,2048]{1,0:T(8,128)(2,1)}, u32[]{:S(2)}) copy-start(bf16[1024,2048]{1,0:T(8,128)(2,1)} %all-gather.7.cloned.1.call-done) | copy-start | bytes 12582916
Sparse Core Ops, SparseCore 0:
  9.8 74.4 all-gather.6
  86.7 135.5 all-gather.4

commit v2 on v1

v2 whole, which is shorter than its diff:
```python
import functools

import jax
import jax.numpy as jnp
from jax import lax
from jax.experimental import pallas as pl
from jax.experimental.pallas import tpu as pltpu
from jax.sharding import PartitionSpec as P

F32, BF16 = jnp.float32, jnp.bfloat16
HC = 128
BLK = 128
CAP = 12
QUARTERS = 4
EPS = 1e-06
LIMIT = 7.0
SLOPE = 1.702
VMEM = pltpu.VMEM
MESH = pl.DeviceIdType.MESH
WHOLE = pl.BlockSpec(memory_space=VMEM)
SLAB = 16
ANYWHERE = pl.BlockSpec(memory_space=pl.ANY)


def mm(a, b):
    return jnp.dot(a, b, preferred_element_type=F32)


def mm_t(a, b):
    return lax.dot_general(a, b, (((1,), (1,)), ((), ())), preferred_element_type=F32)


def t_mm(a, b):
    return lax.dot_general(a, b, (((0,), (0,)), ((), ())), preferred_element_type=F32)


def iota(shape, dim):
    return lax.broadcasted_iota(jnp.int32, shape, dim)


def logistic(x):
    return 1.0 / (1.0 + jnp.exp(-x))


def recurrence_states(q_ref, g_ref, v_ref, margin_ref, pos_ref, qin, kin, before, off, fin, inc, last):
    blocks = q_ref.shape[0] // BLK
    heads = q_ref.shape[1] // HC
    row, col = iota((BLK, BLK), 0), iota((BLK, BLK), 1)
    keep = (row >= col, row <= col)
    tri = [k.astype(BF16) for k in keep]
    ends = [jnp.exp(margin_ref[d : d + 1, :]) for d in range(2)]

    def per_block(n, carry):
        rows = pl.ds(pl.multiple_of(n * BLK, BLK), BLK)
        q = q_ref[rows, :].astype(F32)
        q = q * logistic(q) * HC**-0.5
        shut = logistic(-g_ref[rows, :].astype(F32))
        values = v_ref[rows, :]
        pos = pos_ref[:, rows]
        for d in range(2):
            k = ends[d] * shut
            logs = jnp.log1p(-k)
            high = logs.astype(BF16)
            low = (logs - high.astype(F32)).astype(BF16)
            added = jnp.concatenate(
                [
                    jnp.broadcast_to(
                        jnp.sum(
                            jnp.where(keep[d], pos[h : h + 1, :], 0.0), axis=1, keepdims=True
                        ),
                        (BLK, HC),
                    )
                    for h in range(heads)
                ],
                axis=1,
            )
            cum = mm(tri[d], high) + mm(tri[d], low) + added
            end = cum[BLK - 1 :, :] if d == 0 else cum[:1, :]
            qin[d, rows, :] = (q * jnp.exp(cum)).astype(BF16)
            kin[d, rows, :] = (k * jnp.exp(-cum)).astype(BF16)
            ks = (k * jnp.exp(end - cum)).astype(BF16)
            last[d, n] = end
            for h in range(heads):
                cols = slice(h * HC, (h + 1) * HC)
                inc[d, n, h] = t_mm(values[:, cols], ks[:, cols])
        return carry

    lax.fori_loop(0, blocks, per_block, 0)
    for d in range(2):

        def chain(i, carry):
            n = i if d == 0 else blocks - 1 - i
            offset, states = carry
            off[d, n] = offset
            end = last[d, n]
            decay = jnp.exp(end)
            new = []
            for h in range(heads):
                before[d, n, h] = states[h]
                new.append(states[h] * decay[:, h * HC : (h + 1) * HC] + inc[d, n, h])
            return offset + end, tuple(new)

        zero = tuple(jnp.zeros((HC, HC), F32) for _ in range(heads))
        total, states = lax.fori_loop(0, blocks, chain, (jnp.zeros((1, heads * HC), F32), zero))
        decay = jnp.exp(total)
        for h in range(heads):
            put_state(fin, (0, d * heads + h), states[h], decay[:, h * HC : (h + 1) * HC])


def put_state(ref, at, state, decay):
    slab = iota((SLAB, HC), 0)
    high = decay.astype(BF16).astype(F32)
    ref[(*at, slice(0, HC))] = state.astype(BF16)
    ref[(*at, slice(HC, HC + SLAB))] = jnp.where(
        slab == 0, high, jnp.where(slab == 1, decay - high, 0.0)
    ).astype(BF16)


def get_state(ref, at):
    state = ref[(*at, slice(0, HC))].astype(F32)
    decay = jnp.sum(ref[(*at, slice(HC, HC + SLAB))].astype(F32), axis=0, keepdims=True)
    return state, decay


def recurrence_outputs(qin, kin, v_ref, before, off, entering, gain, out):
    blocks = v_ref.shape[0] // BLK
    heads = v_ref.shape[1] // HC
    per = out.shape[1] // BLK
    row, col = iota((BLK, BLK), 0), iota((BLK, BLK), 1)

    def per_block(n, carry):
        rows = pl.ds(pl.multiple_of(n * BLK, BLK), BLK)
        for h in range(heads):
            cols = slice(h * HC, (h + 1) * HC)
            scores, outer = [], None
            for d in range(2):
                q = qin[d, rows, cols]
                scores.append(mm_t(q, kin[d, rows, cols]))
                state = before[d, n, h] + entering[d * heads + h] * jnp.exp(off[d, n, :, cols])
                part = mm_t(q, state.astype(BF16))
                outer = part if outer is None else outer + part
            both = jnp.where(row >= col, scores[0], 0.0) + jnp.where(row <= col, scores[1], 0.0)
            mix = mm(both.astype(BF16), v_ref[rows, cols]) + outer
            scale = lax.rsqrt(jnp.mean(mix * mix, axis=1, keepdims=True) + EPS)
            inside = pl.ds(pl.multiple_of(n % per * BLK, BLK), BLK)
            out[n // per, inside, cols] = (mix * scale * gain[...]).astype(BF16)
        return carry

    lax.fori_loop(0, blocks, per_block, 0)


def chunk_places(shape, dim):
    at = iota(shape, dim)
    piece = sum((at >= q * CAP).astype(jnp.int32) for q in range(1, QUARTERS))
    return at - piece * CAP, piece


def pack_rows(tok_ref, gain_ref, routes_ref, send):
    x = tok_ref[...].astype(F32)
    count, features = x.shape
    experts, chunk, width = send.shape
    scale = lax.rsqrt(jnp.mean(x * x, axis=1, keepdims=True) + EPS)
    normed = (x * scale * gain_ref[...]).astype(BF16)
    eye = iota((count, count), 0) == iota((count, count), 1)
    routes = routes_ref[...]
    names = iota((experts, count), 0)
    hot = []
    for k in range(2):
        line = jnp.sum(jnp.where(eye, routes[:, k : k + 1].astype(F32), 0.0), axis=0, keepdims=True)
        hot.append((line == names.astype(F32)).astype(F32))
    earlier = (iota((count, count), 0) < iota((count, count), 1)).astype(BF16)
    rank = mm((hot[0] + hot[1]).astype(BF16), earlier)
    base = names.astype(F32) * CAP
    dest = [jnp.sum(hot[k] * (rank + base), axis=0, keepdims=True) for k in range(2)]
    inner, piece = chunk_places((experts, chunk, 1), 1)
    slot = (iota((experts, chunk, 1), 0) * CAP + inner).astype(F32).reshape(experts * chunk, 1)
    piece = piece.reshape(experts * chunk, 1)
    picked = jnp.logical_or(slot == dest[0], slot == dest[1])
    lhs = jnp.concatenate(
        [jnp.where(jnp.logical_and(picked, piece == q), 1.0, 0.0) for q in range(QUARTERS)],
        axis=1,
    ).astype(BF16)
    rhs = jnp.concatenate([normed[:, q * width : (q + 1) * width] for q in range(QUARTERS)], axis=0)
    send[...] = mm(lhs, rhs).astype(BF16).reshape(experts, chunk, width)


def merge_places(routes_ref, lhs, experts, chunk):
    routes = routes_ref[...]
    count = routes.shape[0]
    names = iota((count, experts), 1)
    hot = [(routes[:, k : k + 1] == names).astype(F32) for k in range(2)]
    earlier = (iota((count, count), 0) > iota((count, count), 1)).astype(BF16)
    rank = mm(earlier, (hot[0] + hot[1]).astype(BF16))
    base = names.astype(F32) * CAP
    r = iota((1, experts * chunk), 1).astype(F32)
    expert = jnp.floor((r + 0.5) / chunk)
    rest = r - expert * chunk
    piece = jnp.floor((rest + 0.5) / CAP)
    slot = expert * CAP + rest - piece * CAP
    for k in range(2):
        dest = jnp.sum(hot[k] * (rank + base), axis=1, keepdims=True)
        picked = slot == dest
        for q in range(QUARTERS):
            at = (k * QUARTERS + q) * count
            lhs[at : at + count, :] = jnp.where(
                jnp.logical_and(picked, piece == q), 1.0, 0.0
            ).astype(BF16)


def merge_rows(lhs, ret, weight_ref, out):
    experts, chunk, width = ret.shape
    weight = weight_ref[...]
    count = weight.shape[0]
    rows = ret[...].reshape(experts * chunk, width)
    for q in range(QUARTERS):
        total = None
        for k in range(2):
            at = (k * QUARTERS + q) * count
            part = weight[:, k : k + 1] * mm(lhs[at : at + count, :], rows)
            total = part if total is None else total + part
        out[:, q * width : (q + 1) * width] = total.astype(BF16)


def kernel(
    query, gates, value, margin, position, head_gain, mixer_w, tokens, expert_gain,
    routes, token_w, wg_any, wu_any, wd_any, mixed, merged,
    q_v, g_v, v_v, margin_v, pos_v, hgain_v, tok_v, egain_v, routes_v, token_w_v, wg, wu, wd,
    w_all, qin, kin, before, off, inc, last, fin, near, far, group_state, chip_in, entering,
    heads_out, heads_in, send, rows, parts, relay_l, relay_r, from_l, from_r, total, ret,
    xt, perm, lhs,
    in_sem, zs, zr, xs, xr_l, xr_r, ys, yr, qs, qr, fs, fr, ts, tr,
    mate_s, mate_r, near_s, near_r, far_s, far_r, chip_s, chip_r,
    ws, wr, wys, wyr, wms, wmr, hs, hr,
    *, n_ep, n_tp,
):
    me, t = lax.axis_index("ep"), lax.axis_index("tp")
    n_z = n_ep // 2
    half = n_z // 2
    steps = n_z // 2
    z, c = me // 2, me % 2
    mate = 2 * z + 1 - c
    right, left = (t + 1) % n_tp, (t + n_tp - 1) % n_tp
    opposite = (t + 2) % n_tp
    chunk, width = send.shape[1:]
    heads = v_v.shape[1] // HC

    def offset(b, side):
        o = (steps + 1 - b) % steps
        return o if side == 0 else n_z - o - half * ((steps - o) // steps)

    loads = [
        pltpu.make_async_copy(src, dst, in_sem.at[i])
        for i, (src, dst) in enumerate(
            (
                (tokens, tok_v), (expert_gain, egain_v), (routes, routes_v), (token_w, token_w_v),
                (mixer_w, w_all.at[0]), (query, q_v), (gates, g_v), (value, v_v),
                (margin, margin_v), (position, pos_v), (head_gain, hgain_v),
                (wg_any.at[0], wg), (wu_any.at[0], wu), (wd_any.at[0], wd),
            )
        )
    ]
    for copy in loads:
        copy.start()

    barrier = pltpu.get_barrier_semaphore()

    def greet(j, carry):
        pl.semaphore_signal(
            barrier, inc=1, device_id={"ep": (me + j) % n_ep}, device_id_type=MESH
        )
        return carry

    lax.fori_loop(1, n_ep, greet, 0)
    for other in (left, right, opposite):
        pl.semaphore_signal(barrier, inc=1, device_id={"tp": other}, device_id_type=MESH)
    for copy in loads[:4]:
        copy.wait()
    pack_rows(tok_v, egain_v, routes_v, send)
    size = perm.shape[0]
    row, col = iota((size, size), 0), iota((size, size), 1)
    major = sum((row >= k * chunk).astype(jnp.int32) for k in range(1, 4))
    rest = row - major * chunk
    minor = sum((rest >= k * CAP).astype(jnp.int32) for k in range(1, 4))
    target = minor * chunk + major * CAP + (rest - minor * CAP)
    perm[...] = jnp.where(col == target, 1.0, 0.0).astype(BF16)
    pl.semaphore_wait(barrier, n_ep + n_tp - 2)

    def z_copy(b, side, core):
        other = ((z + offset(b, side)) % n_z) * 2 + core
        return pltpu.make_async_remote_copy(
            src_ref=send.at[other],
            dst_ref=rows.at[0, 4 * b + 2 * side + c],
            send_sem=zs.at[4 * b + 2 * side + core],
            recv_sem=zr.at[4 * b + 2 * side + c],
            device_id={"ep": other},
            device_id_type=MESH,
        )

    def own_in(slot):
        return pltpu.make_async_copy(send.at[me], rows.at[0, slot], zr.at[slot])

    def is_self(b, side, core):
        return jnp.logical_and(jnp.logical_and(b == 1, side == 0), core == c)

    def dispatch(b, carry):
        for side in range(2):
            for core in range(2):
                own = is_self(b, side, core)

                @pl.when(own)
                def _():
                    own_in(4 * b + 2 * side + c).start()

                @pl.when(jnp.logical_not(own))
                def _():
                    z_copy(b, side, core).start()

        return carry

    def x_copy(b, way):
        group = pl.ds(4 * b, 4)
        return pltpu.make_async_remote_copy(
            src_ref=rows.at[0, group],
            dst_ref=rows.at[1 + way, group],
            send_sem=xs.at[way, b],
            recv_sem=(xr_l if way == 0 else xr_r).at[b],
            device_id={"tp": right if way == 0 else left},
            device_id_type=MESH,
        )

    def y_copy(b, way):
        group = pl.ds(4 * b + 2 * way, 2)
        return pltpu.make_async_remote_copy(
            src_ref=rows.at[1 + way, group],
            dst_ref=rows.at[3, group],
            send_sem=ys.at[way, b],
            recv_sem=yr.at[way, b],
            device_id={"tp": right if way == 0 else left},
            device_id_type=MESH,
        )

    def q_copy(b, way):
        return pltpu.make_async_remote_copy(
            src_ref=parts.at[3, pl.ds(4 * b + 2 * way, 2)],
            dst_ref=(relay_l if way == 0 else relay_r).at[pl.ds(2 * b, 2)],
            send_sem=qs.at[way, b],
            recv_sem=qr.at[way, b],
            device_id={"tp": right if way == 0 else left},
            device_id_type=MESH,
        )

    def f_copy(b, way):
        group = pl.ds(4 * b, 4)
        return pltpu.make_async_remote_copy(
            src_ref=parts.at[2 - way, group],
            dst_ref=(from_l if way == 0 else from_r).at[group],
            send_sem=fs.at[way, b],
            recv_sem=fr.at[way, b],
            device_id={"tp": right if way == 0 else left},
            device_id_type=MESH,
        )

    def t_copy(b, side, core):
        other = ((z - offset(b, side) + n_z) % n_z) * 2 + core
        slot = 4 * b + 2 * side + core
        return pltpu.make_async_remote_copy(
            src_ref=total.at[slot],
            dst_ref=ret.at[me],
            send_sem=ts.at[slot],
            recv_sem=tr.at[me],
            device_id={"ep": other},
            device_id_type=MESH,
        )

    def t_arrival(e):
        return pltpu.make_async_copy(total.at[0], ret.at[e], tr.at[e])

    def own_out(slot):
        return pltpu.make_async_copy(total.at[slot], ret.at[me], tr.at[me])

    def arrive(b):
        for k in range(4):
            own_in(4 * b + k).wait()
        x_copy(b, 0).start()
        x_copy(b, 1).start()

    def relay(b):
        for way in range(2):
            x_copy(b, way).wait_recv()
            y_copy(b, way).start()

    def compute(b):
        group = pl.ds(4 * b, 4)
        for way in range(2):
            y_copy(b, way).wait_recv()
        turn = perm[...]
        for w in range(4):
            turned = mm(turn, rows[w, group].reshape(4 * chunk, width)).astype(BF16)
            for q in range(QUARTERS):
                xt[w * chunk : (w + 1) * chunk, q * width : (q + 1) * width] = turned[
                    q * chunk : (q + 1) * chunk
                ]
        x = xt[...]
        gate = jnp.minimum(mm(x, wg[...]), LIMIT)
        up = jnp.clip(mm(x, wu[...]), -LIMIT, LIMIT)
        hidden = ((up + 1.0) * gate / (1.0 + jnp.exp(-SLOPE * gate))).astype(BF16)
        y = mm(hidden, wd[...]).astype(BF16)
        for w in range(4):
            piece = jnp.concatenate(
                [
                    y[w * chunk : (w + 1) * chunk, q * width : (q + 1) * width]
                    for q in range(QUARTERS)
                ],
                axis=0,
            )
            parts[w, group] = mm(turn, piece).astype(BF16).reshape(4, chunk, width)

    def start_sum(b):
        for way in range(2):
            q_copy(b, way).start()

    def pass_sum(b):
        for way in range(2):
            q_copy(b, way).wait_recv()
            group = pl.ds(4 * b + 2 * way, 2)
            carried = (relay_l if way == 0 else relay_r)[pl.ds(2 * b, 2)]
            parts[2 - way, group] = (
                parts[2 - way, group].astype(F32) + carried.astype(F32)
            ).astype(BF16)

    def send_sum(b):
        for way in range(2):
            f_copy(b, way).start()

    def finish(b):
        for way in range(2):
            f_copy(b, way).wait_recv()
        group = pl.ds(4 * b, 4)
        total[group] = (
            parts[0, group].astype(F32) + from_l[group].astype(F32) + from_r[group].astype(F32)
        ).astype(BF16)

    def send_back(b):
        for side in range(2):
            for core in range(2):
                own = is_self(b, side, core)

                @pl.when(own)
                def _():
                    own_out(4 * b + 2 * side + core).start()

                @pl.when(jnp.logical_not(own))
                def _():
                    t_copy(b, side, core).start()


    def w_part(who, core, lo, hi):
        size = w_all.shape[1] // 2
        first = core * size + lo * (size // 2)
        return w_all.at[who, pl.ds(pl.multiple_of(first, size // 2), (hi - lo) * (size // 2))]

    def w_copy(way):
        return pltpu.make_async_remote_copy(
            src_ref=w_part(0, c, 0, 2),
            dst_ref=w_part(1 + way, c, 0, 2),
            send_sem=ws.at[way],
            recv_sem=wr.at[way],
            device_id={"tp": right if way == 0 else left},
            device_id_type=MESH,
        )

    def w_relay(way):
        return pltpu.make_async_remote_copy(
            src_ref=w_part(1 + way, c, way, way + 1),
            dst_ref=w_part(3, c, way, way + 1),
            send_sem=wys.at[way],
            recv_sem=wyr.at[way],
            device_id={"tp": right if way == 0 else left},
            device_id_type=MESH,
        )

    def w_mate(who, core):
        return pltpu.make_async_remote_copy(
            src_ref=w_part(who, core, 0, 2),
            dst_ref=w_part(who, core, 0, 2),
            send_sem=wms.at[who],
            recv_sem=wmr.at[who],
            device_id={"ep": mate},
            device_id_type=MESH,
        )

    p, g = z % 4, z // 4

    def mate_copy():
        return pltpu.make_async_remote_copy(
            src_ref=fin.at[0], dst_ref=fin.at[1], send_sem=mate_s, recv_sem=mate_r,
            device_id={"ep": mate}, device_id_type=MESH,
        )

    def near_copy(s):
        return pltpu.make_async_remote_copy(
            src_ref=near.at[0], dst_ref=near.at[s], send_sem=near_s.at[s], recv_sem=near_r.at[s],
            device_id={"ep": (g * 4 + (p + s) % 4) * 2 + c}, device_id_type=MESH,
        )

    def far_copy(d, s):
        other = (z + 4 * s) % n_z if d == 0 else (z - 4 * s + n_z) % n_z
        return pltpu.make_async_remote_copy(
            src_ref=group_state.at[d], dst_ref=far.at[d, s],
            send_sem=far_s.at[d, s], recv_sem=far_r.at[d, s],
            device_id={"ep": other * 2 + c}, device_id_type=MESH,
        )

    def sends_far(d, s):
        return g + s < n_z // 4 if d == 0 else g >= s

    def hears_far(d, s):
        return g >= s if d == 0 else g + s < n_z // 4

    def chip_copy():
        return pltpu.make_async_remote_copy(
            src_ref=chip_in.at[0], dst_ref=chip_in.at[1], send_sem=chip_s, recv_sem=chip_r,
            device_id={"ep": mate}, device_id_type=MESH,
        )

    def share_chip():
        mate_copy().wait_recv()
        for d in range(2):
            at = d * heads + c
            first, first_decay = get_state(fin, (c if d == 0 else 1 - c, at))
            second, second_decay = get_state(fin, (1 - c if d == 0 else c, at))
            put_state(near, (0, d), first * second_decay + second, first_decay * second_decay)

    def send_chip():
        for s in range(1, 4):
            near_copy(s).start()

    def share_group():
        for s in range(1, 4):
            near_copy(s).wait_recv()
        for d in range(2):
            zero, one = jnp.zeros((HC, HC), F32), jnp.ones((1, HC), F32)
            inside, inside_decay, whole, whole_decay = zero, one, zero, one
            for m in range(4) if d == 0 else range(3, -1, -1):
                state, decay = get_state(near, ((p - m + 4) % 4, d))
                passed = (m < p) if d == 0 else (m > p)
                inside = jnp.where(passed, inside * decay + state, inside)
                inside_decay = jnp.where(passed, inside_decay * decay, inside_decay)
                whole, whole_decay = whole * decay + state, whole_decay * decay
            put_state(group_state, (d,), whole, whole_decay)
            entering[2 * d] = inside
            entering[2 * d + 1, 0:8] = jnp.broadcast_to(inside_decay, (8, HC))
        for d in range(2):
            for s in range(1, n_z // 4):

                @pl.when(sends_far(d, s))
                def _():
                    far_copy(d, s).start()

    def share_all():
        for d in range(2):
            inside, inside_decay = entering[2 * d], entering[2 * d + 1, 0:1]
            entering[2 * d + 1] = jnp.zeros((HC, HC), F32)
            for s in range(n_z // 4 - 1, 0, -1):

                @pl.when(hears_far(d, s))
                def _():
                    far_copy(d, s).wait_recv()
                    state, decay = get_state(far, (d, s))
                    entering[2 * d + 1] = entering[2 * d + 1] * decay + state

            chip_in[0, d] = (entering[2 * d + 1] * inside_decay + inside).astype(BF16)
        chip_copy().start()

    def enter():
        chip_copy().wait_recv()
        for d in range(2):
            for h in range(heads):
                at = d * heads + h
                state = chip_in[(h + c) % 2, d].astype(F32)
                other, decay = get_state(fin, (1, at))
                passed = (c == 1) if d == 0 else (c == 0)
                entering[at] = jnp.where(passed, state * decay + other, state)

    def head_copy(k):
        to = (right, left, opposite)[k]
        return pltpu.make_async_remote_copy(
            src_ref=heads_out.at[to], dst_ref=heads_in.at[k],
            send_sem=hs.at[k], recv_sem=hr.at[k],
            device_id={"tp": to}, device_id_type=MESH,
        )

    ahead = 3
    lax.fori_loop(0, ahead, dispatch, 0)
    for copy in loads[4:]:
        copy.wait()
    w_copy(0).start()
    w_copy(1).start()
    recurrence_states(q_v, g_v, v_v, margin_v, pos_v, qin, kin, before, off, fin, inc, last)
    mate_copy().start()

    def body(i, carry):
        def stage(lag, fn, until=steps):
            @pl.when(jnp.logical_and(i >= lag, i < until + lag))
            def _():
                fn(i - lag)

        def once(at, fn):
            @pl.when(i == at)
            def _():
                fn()

        def relay_weights():
            for way in range(2):
                w_copy(way).wait_recv()
                w_relay(way).start()

        def pair_weights():
            for way in range(2):
                w_relay(way).wait_recv()
            for who in range(1, 4):
                w_mate(who, c).start()

        stage(4, finish)
        stage(3, pass_sum)
        stage(2, compute)
        stage(4, send_back)
        stage(3, send_sum)
        stage(1, relay)
        stage(2, start_sum)
        once(0, share_chip)
        stage(0, arrive)
        once(0, send_chip)
        once(1, relay_weights)
        once(3, share_group)
        stage(0, lambda b: dispatch(b + ahead, 0), steps - ahead)
        once(4, pair_weights)
        once(6, share_all)
        return carry

    lax.fori_loop(0, steps + 4, body, 0)

    enter()
    recurrence_outputs(qin, kin, v_v, before, off, entering, hgain_v, heads_out)
    for k in range(3):
        head_copy(k).start()
    merge_places(routes_v, lhs, n_ep, chunk)
    for who in range(1, 4):
        w_mate(who, 1 - c).wait_recv()
    for k in range(3):
        head_copy(k).wait_recv()
    span = mixed.shape[1] // 4
    for k in range(4):
        cols = slice(k * span, (k + 1) * span)
        acc = None
        for who in range(4):
            own = heads_out[t] if who == 0 else heads_in[who - 1]
            part = mm(own, w_all[who, :, cols]).astype(BF16).astype(F32)
            acc = part if acc is None else acc + part
        mixed[:, cols] = acc.astype(BF16)

    def returned(e, carry):
        t_arrival(e).wait()
        return carry

    lax.fori_loop(0, n_ep, returned, 0)
    merge_rows(lhs, ret, token_w_v, merged)

    def sent(b, carry):
        for way in range(2):
            x_copy(b, way).wait_send()
            y_copy(b, way).wait_send()
            q_copy(b, way).wait_send()
            f_copy(b, way).wait_send()
        for side in range(2):
            for core in range(2):

                @pl.when(jnp.logical_not(is_self(b, side, core)))
                def _():
                    z_copy(b, side, core).wait_send()
                    t_copy(b, side, core).wait_send()

        return carry

    lax.fori_loop(0, steps, sent, 0)
    for way in range(2):
        w_copy(way).wait_send()
        w_relay(way).wait_send()
    for s in range(1, 4):
        w_mate(s, c).wait_send()
        near_copy(s).wait_send()
    for d in range(2):
        for s in range(1, n_z // 4):

            @pl.when(sends_far(d, s))
            def _():
                far_copy(d, s).wait_send()

    mate_copy().wait_send()
    chip_copy().wait_send()
    for k in range(3):
        head_copy(k).wait_send()


def body(*args):
    (query, gates, value, margin, position, head_gain, mixer_w, tokens, expert_gain,
     routes, token_w, wg, wu, wd) = args
    n_ep, n_tp = lax.axis_size("ep"), lax.axis_size("tp")
    length, channels = query.shape
    heads, blocks = channels // HC, length // BLK
    count, features = tokens.shape
    chunk, width = CAP * QUARTERS, features // QUARTERS
    many = (n_ep, chunk, width)
    half_many = (n_ep // 2, chunk, width)
    steps = n_ep // 4
    group = 4 * chunk
    dma = pltpu.SemaphoreType.DMA
    operands = (
        query, gates, value, margin, position, head_gain[None, :], mixer_w, tokens,
        expert_gain[None, :], routes, token_w, wg, wu, wd,
    )

    def like(x):
        return VMEM(x.shape, x.dtype)

    per_block = (2, blocks, heads, HC, HC)
    lines = (2, blocks, 1, channels)
    state = (HC + SLAB, HC)
    mixed, merged = pl.pallas_call(
        functools.partial(kernel, n_ep=n_ep, n_tp=n_tp),
        out_shape=(
            jax.ShapeDtypeStruct((length // n_tp, features), BF16),
            jax.ShapeDtypeStruct((count, features), BF16),
        ),
        in_specs=[ANYWHERE] * len(operands),
        out_specs=(WHOLE, WHOLE),
        scratch_shapes=[
            like(query), like(gates), like(value), like(margin), like(position),
            like(operands[5]), like(tokens), like(operands[8]), like(routes), like(token_w),
            VMEM(wg.shape[1:], BF16), VMEM(wu.shape[1:], BF16), VMEM(wd.shape[1:], BF16),
            VMEM((n_tp, *mixer_w.shape), BF16),
            VMEM((2, length, channels), BF16), VMEM((2, length, channels), BF16),
            VMEM(per_block, F32), VMEM(lines, F32), VMEM(per_block, F32), VMEM(lines, F32),
            VMEM((2, 2 * heads, *state), BF16),
            VMEM((4, 2, *state), BF16), VMEM((2, 4, *state), BF16), VMEM((2, *state), BF16),
            VMEM((2, 2, HC, HC), BF16), VMEM((2 * heads, HC, HC), F32),
            VMEM((n_tp, length // n_tp, channels), BF16),
            VMEM((3, length // n_tp, channels), BF16),
            VMEM(many, BF16), VMEM((4, *many), BF16), VMEM((4, *many), BF16),
            VMEM(half_many, BF16), VMEM(half_many, BF16),
            VMEM(many, BF16), VMEM(many, BF16), VMEM(many, BF16), VMEM(many, BF16),
            VMEM((group, features), BF16), VMEM((group, group), BF16),
            VMEM((2 * QUARTERS * count, n_ep * chunk), BF16),
            dma((len(operands),)),
            dma((n_ep,)), dma((n_ep,)),
            dma((2, steps)), dma((steps,)), dma((steps,)),
            dma((2, steps)), dma((2, steps)),
            dma((2, steps)), dma((2, steps)),
            dma((2, steps)), dma((2, steps)),
            dma((n_ep,)), dma((n_ep,)),
            dma(()), dma(()), dma((4,)), dma((4,)), dma((2, 4)), dma((2, 4)), dma(()), dma(()),
            dma((2,)), dma((2,)), dma((2,)), dma((2,)), dma((4,)), dma((4,)),
            dma((3,)), dma((3,)),
        ],
        compiler_params=pltpu.CompilerParams(
            collective_id=0, has_side_effects=True, vmem_limit_bytes=62 * 2**20
        ),
        name="whole",
    )(*operands)
    return mixed, merged


def solution(mesh):
    rows = P(("grp", "ep"), "tp")
    split = P(("grp", "ep", "tp"), None)
    return jax.shard_map(
        body,
        mesh=mesh,
        in_specs=(
            rows, rows, rows, P(None, "tp"), P("tp", ("grp", "ep")), P(), P("tp", None),
            split, P(), split, split,
            P("ep", None, "tp"), P("ep", None, "tp"), P("ep", "tp", None),
        ),
        out_specs=(split, split),
        check_vma=False,
    )
```

time: 260 us -> 195 us (0.75)
  Pallas kernels: 206 us -> 188 us
  between operations: 14.2 us -> 0.65 us
  local copies, waits for them, and re-layouts: 18.2 us -> 5.99 us
  waiting for transfers between devices: 10.6 us -> 0 us
  matrix products: 5.41 us -> 0 us
  starting transfers between devices: 4.15 us -> 0 us
    pallas_call x5 -> x1, Pallas kernels: 206 us -> 188 us  [body(): pl.pallas_call(functools.partial(kernel, n_ep=n_ep, n_tp=n_tp), out_shape...]
    unnamed x45 -> x6, local copies, waits for them, and re-layouts: 18.2 us -> 5.99 us
    dot_general x4 -> x0, matrix products: 5.41 us -> none  [mm(): return jnp.dot(a, b, preferred_element_type=F32)]
    all_gather x2 -> x0, waiting for transfers between devices: 5.38 us -> none  [the longest x1 5.36 us: body(): every = lax.all_gather(fin, 'ep')]
    all_to_all x1 -> x0, waiting for transfers between devices: 4.46 us -> none  [body(): lax.all_to_all(heads_out.reshape(n_tp, length // n_tp, channels), 'tp', 0...]
    all_to_all x1 -> x0, starting transfers between devices: 4.02 us -> none  [body(): lax.all_to_all(heads_out.reshape(n_tp, length // n_tp, channels), 'tp', 0...]
  transfers between devices with their start and end apart: 3 -> 0, of which waited for: 2 -> 0; matrix products, arithmetic and copies ran while one was open for 1% -> 0% of each run, Pallas kernels for 77% -> 0%
where the time goes in v2:
time: 195 us
  Pallas kernels  188 us (96%)
  local copies, waits for them, and re-layouts  5.99 us (3%)
    pallas_call x1, Pallas kernels, body(): pl.pallas_call(functools.partial(kernel, n_ep=n_ep, n_tp=n_tp), out_shape...  188 us
    unnamed x6, local copies, waits for them, and re-layouts  5.99 us

profile of v2, /device:TPU:33, one launch (start us, length us, event | category | flops | bytes accessed | tf_op | source)
XLA Modules:
  0.0 194.5 jit_solution(10823207677534468170)
XLA Ops:
  0.6 1.4 copy.16.routes
  2.0 1.4 copy.17.token_w
  3.5 187.9 %whole.1 = (bf16[256,2048]{1,0:T(8,128)(2,1)}, bf16[128,2048]{1,0:T(8,128)(2,1)}) custom-call(bf16[1024,256]{1,0:T(8,128)(2,1)} %query.1, bf16[1024,256]{1,0:T(8,128)(2,1)} %gates.1, bf16[1024,256]{1,0:T(8,128)(2,1)} %value.1, f32[2,256]{1,0:T(2,128)} %margin.1, f32[2,1024]{1,0:T(2,128)} %position.1, f32[1,128]{1,0:T(1,128)} %bitcast.3, ...), custom_call_target="tpu_custom_call" | custom-call | tf_op jit(solution)/shard_map/whole/pallas_call | solution.py:729
  191.4 0.0 copy-start
  191.4 2.4 %copy.20 = bf16[256,2048]{1,0:T(8,128)(2,1)} copy(bf16[256,2048]{1,0:T(8,128)(2,1)} %get-tuple-element.4) | data formatting | bytes 2097152
  193.7 0.0 copy-done
  193.7 0.8 copy.21
Async XLA Ops:
  191.4 2.4 %copy-start = (bf16[128,2048]{1,0:T(8,128)(2,1)S(1)}, bf16[128,2048]{1,0:T(8,128)(2,1)}, u32[]{:S(2)}) copy-start(bf16[128,2048]{1,0:T(8,128)(2,1)} %get-tuple-element.5) | copy-start | bytes 1572868

commit v3 on v2

--- a/solution.py
+++ b/solution.py
@@ -161,13 +161,9 @@
     experts, chunk, width = send.shape
     scale = lax.rsqrt(jnp.mean(x * x, axis=1, keepdims=True) + EPS)
     normed = (x * scale * gain_ref[...]).astype(BF16)
-    eye = iota((count, count), 0) == iota((count, count), 1)
     routes = routes_ref[...]
     names = iota((experts, count), 0)
-    hot = []
-    for k in range(2):
-        line = jnp.sum(jnp.where(eye, routes[:, k : k + 1].astype(F32), 0.0), axis=0, keepdims=True)
-        hot.append((line == names.astype(F32)).astype(F32))
+    hot = [(routes[k : k + 1, :] == names).astype(F32) for k in range(2)]
     earlier = (iota((count, count), 0) < iota((count, count), 1)).astype(BF16)
     rank = mm((hot[0] + hot[1]).astype(BF16), earlier)
     base = names.astype(F32) * CAP
@@ -184,39 +180,53 @@
     send[...] = mm(lhs, rhs).astype(BF16).reshape(experts, chunk, width)
 
 
-def merge_places(routes_ref, lhs, experts, chunk):
-    routes = routes_ref[...]
-    count = routes.shape[0]
-    names = iota((count, experts), 1)
-    hot = [(routes[:, k : k + 1] == names).astype(F32) for k in range(2)]
+def as_column(line):
+    count = line.shape[1]
+    eye = iota((count, count), 0) == iota((count, count), 1)
+    return jnp.sum(jnp.where(eye, line, 0.0), axis=1, keepdims=True)
+
+
+def merge_places(routes_ref, lhs, chunk, expert_of):
+    count = routes_ref.shape[1]
+    rows = lhs.shape[1]
+    experts = rows // chunk
+    routes = routes_ref[...].astype(F32)
+    names = iota((count, experts), 1).astype(F32)
+    hot = [(as_column(routes[k : k + 1, :]) == names).astype(F32) for k in range(2)]
     earlier = (iota((count, count), 0) > iota((count, count), 1)).astype(BF16)
     rank = mm(earlier, (hot[0] + hot[1]).astype(BF16))
-    base = names.astype(F32) * CAP
-    r = iota((1, experts * chunk), 1).astype(F32)
-    expert = jnp.floor((r + 0.5) / chunk)
-    rest = r - expert * chunk
+    base = names * CAP
+    r = iota((1, rows), 1).astype(F32)
+    at = jnp.floor((r + 0.5) / chunk)
+    rest = r - at * chunk
     piece = jnp.floor((rest + 0.5) / CAP)
-    slot = expert * CAP + rest - piece * CAP
+    slot = expert_of(at) * CAP + rest - piece * CAP
     for k in range(2):
         dest = jnp.sum(hot[k] * (rank + base), axis=1, keepdims=True)
         picked = slot == dest
         for q in range(QUARTERS):
-            at = (k * QUARTERS + q) * count
-            lhs[at : at + count, :] = jnp.where(
+            first = (k * QUARTERS + q) * count
+            lhs[first : first + count, :] = jnp.where(
                 jnp.logical_and(picked, piece == q), 1.0, 0.0
             ).astype(BF16)
 
 
-def merge_rows(lhs, ret, weight_ref, out):
+def merge_early(lhs, ret, early, cut):
+    chunk, width = ret.shape[1:]
+    rows = ret[:cut].reshape(cut * chunk, width)
+    early[...] = mm(lhs[:, : cut * chunk], rows)
+
+
+def merge_rows(lhs, ret, early, cut, weight_ref, out):
     experts, chunk, width = ret.shape
-    weight = weight_ref[...]
-    count = weight.shape[0]
-    rows = ret[...].reshape(experts * chunk, width)
+    count = weight_ref.shape[1]
+    weight = [as_column(weight_ref[k : k + 1, :]) for k in range(2)]
+    rows = ret[cut:].reshape((experts - cut) * chunk, width)
     for q in range(QUARTERS):
         total = None
         for k in range(2):
-            at = (k * QUARTERS + q) * count
-            part = weight[:, k : k + 1] * mm(lhs[at : at + count, :], rows)
+            span = slice((k * QUARTERS + q) * count, (k * QUARTERS + q + 1) * count)
+            part = weight[k] * (early[span, :] + mm(lhs[span, cut * chunk :], rows))
             total = part if total is None else total + part
         out[:, q * width : (q + 1) * width] = total.astype(BF16)
 
@@ -227,9 +237,9 @@
     q_v, g_v, v_v, margin_v, pos_v, hgain_v, tok_v, egain_v, routes_v, token_w_v, wg, wu, wd,
     w_all, qin, kin, before, off, inc, last, fin, near, far, group_state, chip_in, entering,
     heads_out, heads_in, send, rows, parts, relay_l, relay_r, from_l, from_r, total, ret,
-    xt, perm, lhs,
+    xt, perm, lhs, early, lead, ahead_state,
     in_sem, zs, zr, xs, xr_l, xr_r, ys, yr, qs, qr, fs, fr, ts, tr,
-    mate_s, mate_r, near_s, near_r, far_s, far_r, chip_s, chip_r,
+    mate_s, mate_r, near_s, near_r, far_s, far_r, lead_s, lead_r, chip_s, chip_r,
     ws, wr, wys, wyr, wms, wmr, hs, hr,
     *, n_ep, n_tp,
 ):
@@ -276,13 +286,6 @@
     for copy in loads[:4]:
         copy.wait()
     pack_rows(tok_v, egain_v, routes_v, send)
-    size = perm.shape[0]
-    row, col = iota((size, size), 0), iota((size, size), 1)
-    major = sum((row >= k * chunk).astype(jnp.int32) for k in range(1, 4))
-    rest = row - major * chunk
-    minor = sum((rest >= k * CAP).astype(jnp.int32) for k in range(1, 4))
-    target = minor * chunk + major * CAP + (rest - minor * CAP)
-    perm[...] = jnp.where(col == target, 1.0, 0.0).astype(BF16)
     pl.semaphore_wait(barrier, n_ep + n_tp - 2)
 
     def z_copy(b, side, core):
@@ -365,9 +368,9 @@
         slot = 4 * b + 2 * side + core
         return pltpu.make_async_remote_copy(
             src_ref=total.at[slot],
-            dst_ref=ret.at[me],
+            dst_ref=ret.at[4 * b + 2 * side + c],
             send_sem=ts.at[slot],
-            recv_sem=tr.at[me],
+            recv_sem=tr.at[4 * b + 2 * side + c],
             device_id={"ep": other},
             device_id_type=MESH,
         )
@@ -376,7 +379,7 @@
         return pltpu.make_async_copy(total.at[0], ret.at[e], tr.at[e])
 
     def own_out(slot):
-        return pltpu.make_async_copy(total.at[slot], ret.at[me], tr.at[me])
+        return pltpu.make_async_copy(total.at[slot], ret.at[slot], tr.at[slot])
 
     def arrive(b):
         for k in range(4):
@@ -497,10 +500,29 @@
             device_id={"ep": mate}, device_id_type=MESH,
         )
 
-    def near_copy(s):
-        return pltpu.make_async_remote_copy(
-            src_ref=near.at[0], dst_ref=near.at[s], send_sem=near_s.at[s], recv_sem=near_r.at[s],
-            device_id={"ep": (g * 4 + (p + s) % 4) * 2 + c}, device_id_type=MESH,
+    def near_copy(d, s):
+        other = z + s if d == 0 else z - s
+        return pltpu.make_async_remote_copy(
+            src_ref=near.at[0, d], dst_ref=near.at[s, d],
+            send_sem=near_s.at[d, s], recv_sem=near_r.at[d, s],
+            device_id={"ep": (other + n_z) % n_z * 2 + c}, device_id_type=MESH,
+        )
+
+    def sends_near(d, s):
+        return p + s < 4 if d == 0 else p >= s
+
+    def hears_near(d, s):
+        return p >= s if d == 0 else p + s < 4
+
+    def leads(d):
+        return p == 3 if d == 0 else p == 0
+
+    def lead_copy(d, s):
+        other = z - s if d == 0 else z + s
+        return pltpu.make_async_remote_copy(
+            src_ref=lead.at[d], dst_ref=lead.at[d],
+            send_sem=lead_s.at[d, s], recv_sem=lead_r.at[d],
+            device_id={"ep": (other + n_z) % n_z * 2 + c}, device_id_type=MESH,
         )
 
     def far_copy(d, s):
@@ -512,10 +534,10 @@
         )
 
     def sends_far(d, s):
-        return g + s < n_z // 4 if d == 0 else g >= s
+        return jnp.logical_and(leads(d), g + s < n_z // 4 if d == 0 else g >= s)
 
     def hears_far(d, s):
-        return g >= s if d == 0 else g + s < n_z // 4
+        return jnp.logical_and(leads(d), g >= s if d == 0 else g + s < n_z // 4)
 
     def chip_copy():
         return pltpu.make_async_remote_copy(
@@ -532,24 +554,30 @@
             put_state(near, (0, d), first * second_decay + second, first_decay * second_decay)
 
     def send_chip():
-        for s in range(1, 4):
-            near_copy(s).start()
+        for d in range(2):
+            for s in range(1, 4):
+
+                @pl.when(sends_near(d, s))
+                def _():
+                    near_copy(d, s).start()
 
     def share_group():
-        for s in range(1, 4):
-            near_copy(s).wait_recv()
-        for d in range(2):
-            zero, one = jnp.zeros((HC, HC), F32), jnp.ones((1, HC), F32)
-            inside, inside_decay, whole, whole_decay = zero, one, zero, one
-            for m in range(4) if d == 0 else range(3, -1, -1):
-                state, decay = get_state(near, ((p - m + 4) % 4, d))
-                passed = (m < p) if d == 0 else (m > p)
-                inside = jnp.where(passed, inside * decay + state, inside)
-                inside_decay = jnp.where(passed, inside_decay * decay, inside_decay)
-                whole, whole_decay = whole * decay + state, whole_decay * decay
-            put_state(group_state, (d,), whole, whole_decay)
-            entering[2 * d] = inside
-            entering[2 * d + 1, 0:8] = jnp.broadcast_to(inside_decay, (8, HC))
+        for d in range(2):
+            entering[2 * d] = jnp.zeros((HC, HC), F32)
+            entering[2 * d + 1, 0:8] = jnp.ones((8, HC), F32)
+            for s in range(3, 0, -1):
+
+                @pl.when(hears_near(d, s))
+                def _():
+                    near_copy(d, s).wait_recv()
+                    state, decay = get_state(near, (s, d))
+                    entering[2 * d] = entering[2 * d] * decay + state
+                    entering[2 * d + 1, 0:8] = entering[2 * d + 1, 0:8] * decay
+
+            state, decay = get_state(near, (0, d))
+            put_state(
+                group_state, (d,), entering[2 * d] * decay + state, entering[2 * d + 1, 0:1] * decay
+            )
         for d in range(2):
             for s in range(1, n_z // 4):
 
@@ -557,19 +585,40 @@
                 def _():
                     far_copy(d, s).start()
 
-    def share_all():
-        for d in range(2):
-            inside, inside_decay = entering[2 * d], entering[2 * d + 1, 0:1]
-            entering[2 * d + 1] = jnp.zeros((HC, HC), F32)
+    def share_far():
+        for d in range(2):
+            ahead_state[d] = jnp.zeros((HC, HC), F32)
             for s in range(n_z // 4 - 1, 0, -1):
 
                 @pl.when(hears_far(d, s))
                 def _():
                     far_copy(d, s).wait_recv()
                     state, decay = get_state(far, (d, s))
-                    entering[2 * d + 1] = entering[2 * d + 1] * decay + state
-
-            chip_in[0, d] = (entering[2 * d + 1] * inside_decay + inside).astype(BF16)
+                    ahead_state[d] = ahead_state[d] * decay + state
+
+        for d in range(2):
+
+            @pl.when(leads(d))
+            def _():
+                lead[d] = ahead_state[d].astype(BF16)
+
+        for d in range(2):
+            for s in range(1, 4):
+
+                @pl.when(leads(d))
+                def _():
+                    lead_copy(d, s).start()
+
+    def share_all():
+        for d in range(2):
+
+            @pl.when(jnp.logical_not(leads(d)))
+            def _():
+                lead_copy(d, 1).wait_recv()
+
+            chip_in[0, d] = (
+                lead[d].astype(F32) * entering[2 * d + 1, 0:1] + entering[2 * d]
+            ).astype(BF16)
         chip_copy().start()
 
     def enter():
@@ -590,12 +639,30 @@
             device_id={"tp": to}, device_id_type=MESH,
         )
 
+    def expert_of(at):
+        b = jnp.floor((at + 0.5) / 4)
+        side = jnp.floor((at - 4 * b + 0.5) / 2)
+        core = at - 4 * b - 2 * side
+        o = steps + 1 - b
+        o = o - steps * jnp.floor((o + 0.5) / steps)
+        other = jnp.where(side < 0.5, o, n_z - o - jnp.where(o < 0.5, 1.0 * half, 0.0))
+        other = other + z.astype(F32)
+        other = other - n_z * jnp.floor((other + 0.5) / n_z)
+        return 2 * other + core
+
     ahead = 3
     lax.fori_loop(0, ahead, dispatch, 0)
     for copy in loads[4:]:
         copy.wait()
     w_copy(0).start()
     w_copy(1).start()
+    size = perm.shape[0]
+    row, col = iota((size, size), 0), iota((size, size), 1)
+    major = sum((row >= k * chunk).astype(jnp.int32) for k in range(1, 4))
+    rest = row - major * chunk
+    minor = sum((rest >= k * CAP).astype(jnp.int32) for k in range(1, 4))
+    target = minor * chunk + major * CAP + (rest - minor * CAP)
+    perm[...] = jnp.where(col == target, 1.0, 0.0).astype(BF16)
     recurrence_states(q_v, g_v, v_v, margin_v, pos_v, qin, kin, before, off, fin, inc, last)
     mate_copy().start()
 
@@ -635,16 +702,17 @@
         once(3, share_group)
         stage(0, lambda b: dispatch(b + ahead, 0), steps - ahead)
         once(4, pair_weights)
-        once(6, share_all)
+        once(6, share_far)
         return carry
 
     lax.fori_loop(0, steps + 4, body, 0)
 
+    share_all()
+    merge_places(routes_v, lhs, chunk, expert_of)
     enter()
     recurrence_outputs(qin, kin, v_v, before, off, entering, hgain_v, heads_out)
     for k in range(3):
         head_copy(k).start()
-    merge_places(routes_v, lhs, n_ep, chunk)
     for who in range(1, 4):
         w_mate(who, 1 - c).wait_recv()
     for k in range(3):
@@ -663,8 +731,11 @@
         t_arrival(e).wait()
         return carry
 
-    lax.fori_loop(0, n_ep, returned, 0)
-    merge_rows(lhs, ret, token_w_v, merged)
+    cut = n_ep - 8
+    lax.fori_loop(0, cut, returned, 0)
+    merge_early(lhs, ret, early, cut)
+    lax.fori_loop(cut, n_ep, returned, 0)
+    merge_rows(lhs, ret, early, cut, token_w_v, merged)
 
     def sent(b, carry):
         for way in range(2):
@@ -686,10 +757,19 @@
     for way in range(2):
         w_copy(way).wait_send()
         w_relay(way).wait_send()
-    for s in range(1, 4):
-        w_mate(s, c).wait_send()
-        near_copy(s).wait_send()
+    for who in range(1, 4):
+        w_mate(who, c).wait_send()
     for d in range(2):
+        for s in range(1, 4):
+
+            @pl.when(sends_near(d, s))
+            def _():
+                near_copy(d, s).wait_send()
+
+            @pl.when(leads(d))
+            def _():
+                lead_copy(d, s).wait_send()
+
         for s in range(1, n_z // 4):
 
             @pl.when(sends_far(d, s))
@@ -717,7 +797,7 @@
     dma = pltpu.SemaphoreType.DMA
     operands = (
         query, gates, value, margin, position, head_gain[None, :], mixer_w, tokens,
-        expert_gain[None, :], routes, token_w, wg, wu, wd,
+        expert_gain[None, :], jnp.transpose(routes), jnp.transpose(token_w), wg, wu, wd,
     )
 
     def like(x):
@@ -736,7 +816,7 @@
         out_specs=(WHOLE, WHOLE),
         scratch_shapes=[
             like(query), like(gates), like(value), like(margin), like(position),
-            like(operands[5]), like(tokens), like(operands[8]), like(routes), like(token_w),
+            like(operands[5]), like(tokens), like(operands[8]), like(operands[9]), like(operands[10]),
             VMEM(wg.shape[1:], BF16), VMEM(wu.shape[1:], BF16), VMEM(wd.shape[1:], BF16),
             VMEM((n_tp, *mixer_w.shape), BF16),
             VMEM((2, length, channels), BF16), VMEM((2, length, channels), BF16),
@@ -751,6 +831,8 @@
             VMEM(many, BF16), VMEM(many, BF16), VMEM(many, BF16), VMEM(many, BF16),
             VMEM((group, features), BF16), VMEM((group, group), BF16),
             VMEM((2 * QUARTERS * count, n_ep * chunk), BF16),
+            VMEM((2 * QUARTERS * count, width), F32),
+            VMEM((2, HC, HC), BF16), VMEM((2, HC, HC), F32),
             dma((len(operands),)),
             dma((n_ep,)), dma((n_ep,)),
             dma((2, steps)), dma((steps,)), dma((steps,)),
@@ -758,7 +840,8 @@
             dma((2, steps)), dma((2, steps)),
             dma((2, steps)), dma((2, steps)),
             dma((n_ep,)), dma((n_ep,)),
-            dma(()), dma(()), dma((4,)), dma((4,)), dma((2, 4)), dma((2, 4)), dma(()), dma(()),
+            dma(()), dma(()), dma((2, 4)), dma((2, 4)), dma((2, 4)), dma((2, 4)),
+            dma((2, 4)), dma((2,)), dma(()), dma(()),
             dma((2,)), dma((2,)), dma((2,)), dma((2,)), dma((4,)), dma((4,)),
             dma((3,)), dma((3,)),
         ],

time: 195 us -> 187 us (0.959)
  Pallas kernels: 188 us -> 183 us
  local copies, waits for them, and re-layouts: 5.99 us -> 3.16 us
    pallas_call x1, Pallas kernels: 188 us -> 183 us  [body(): pl.pallas_call(functools.partial(kernel, n_ep=n_ep, n_tp=n_tp), out_shape...]
    unnamed x6 -> x4, local copies, waits for them, and re-layouts: 5.99 us -> 3.16 us
where the time goes in v3:
time: 187 us; the launch traced here: 186 us
  Pallas kernels  183 us (98%)
  local copies, waits for them, and re-layouts  3.16 us (2%)
    pallas_call x1, Pallas kernels, body(): pl.pallas_call(functools.partial(kernel, n_ep=n_ep, n_tp=n_tp), out_shape...  183 us

profile of v3, /device:TPU:33, one launch (start us, length us, event | category | flops | bytes accessed | tf_op | source)
XLA Modules:
  0.0 186.5 jit_solution(2282373500897854468)
XLA Ops:
  0.6 182.7 %whole.1 = (bf16[256,2048]{1,0:T(8,128)(2,1)}, bf16[128,2048]{1,0:T(8,128)(2,1)}) custom-call(bf16[1024,256]{1,0:T(8,128)(2,1)} %query.1, bf16[1024,256]{1,0:T(8,128)(2,1)} %gates.1, bf16[1024,256]{1,0:T(8,128)(2,1)} %value.1, f32[2,256]{1,0:T(2,128)} %margin.1, f32[2,1024]{1,0:T(2,128)} %position.1, f32[1,128]{1,0:T(1,128)} %bitcast.7, ...), custom_call_target="tpu_custom_call" | custom-call | tf_op jit(solution)/shard_map/whole/pallas_call | solution.py:809
  183.3 0.0 copy-start
  183.3 2.4 %copy.18 = bf16[256,2048]{1,0:T(8,128)(2,1)} copy(bf16[256,2048]{1,0:T(8,128)(2,1)} %get-tuple-element.4) | data formatting | bytes 2097152
  185.7 0.0 copy-done
  185.7 0.8 copy.19
Async XLA Ops:
  183.3 2.4 %copy-start = (bf16[128,2048]{1,0:T(8,128)(2,1)S(1)}, bf16[128,2048]{1,0:T(8,128)(2,1)}, u32[]{:S(2)}) copy-start(bf16[128,2048]{1,0:T(8,128)(2,1)} %get-tuple-element.5) | copy-start | bytes 1572868

commit v4 on v3

--- a/solution.py
+++ b/solution.py
@@ -247,6 +247,7 @@
     n_z = n_ep // 2
     half = n_z // 2
     steps = n_z // 2
+    self_step = steps // 2 - 1
     z, c = me // 2, me % 2
     mate = 2 * z + 1 - c
     right, left = (t + 1) % n_tp, (t + n_tp - 1) % n_tp
@@ -255,7 +256,7 @@
     heads = v_v.shape[1] // HC
 
     def offset(b, side):
-        o = (steps + 1 - b) % steps
+        o = (steps + self_step - b) % steps
         return o if side == 0 else n_z - o - half * ((steps - o) // steps)
 
     loads = [
@@ -303,7 +304,7 @@
         return pltpu.make_async_copy(send.at[me], rows.at[0, slot], zr.at[slot])
 
     def is_self(b, side, core):
-        return jnp.logical_and(jnp.logical_and(b == 1, side == 0), core == c)
+        return jnp.logical_and(jnp.logical_and(b == self_step, side == 0), core == c)
 
     def dispatch(b, carry):
         for side in range(2):
@@ -408,7 +409,7 @@
         up = jnp.clip(mm(x, wu[...]), -LIMIT, LIMIT)
         hidden = ((up + 1.0) * gate / (1.0 + jnp.exp(-SLOPE * gate))).astype(BF16)
         y = mm(hidden, wd[...]).astype(BF16)
-        for w in range(4):
+        for w in (3, 2, 1, 0):
             piece = jnp.concatenate(
                 [
                     y[w * chunk : (w + 1) * chunk, q * width : (q + 1) * width]
@@ -643,14 +644,14 @@
         b = jnp.floor((at + 0.5) / 4)
         side = jnp.floor((at - 4 * b + 0.5) / 2)
         core = at - 4 * b - 2 * side
-        o = steps + 1 - b
+        o = steps + self_step - b
         o = o - steps * jnp.floor((o + 0.5) / steps)
         other = jnp.where(side < 0.5, o, n_z - o - jnp.where(o < 0.5, 1.0 * half, 0.0))
         other = other + z.astype(F32)
         other = other - n_z * jnp.floor((other + 0.5) / n_z)
         return 2 * other + core
 
-    ahead = 3
+    ahead = 4
     lax.fori_loop(0, ahead, dispatch, 0)
     for copy in loads[4:]:
         copy.wait()
@@ -688,12 +689,12 @@
             for who in range(1, 4):
                 w_mate(who, c).start()
 
+        stage(3, pass_sum)
         stage(4, finish)
-        stage(3, pass_sum)
-        stage(2, compute)
-        stage(4, send_back)
         stage(3, send_sum)
         stage(1, relay)
+        stage(4, send_back)
+        stage(2, compute)
         stage(2, start_sum)
         once(0, share_chip)
         stage(0, arrive)
@@ -809,8 +810,8 @@
     mixed, merged = pl.pallas_call(
         functools.partial(kernel, n_ep=n_ep, n_tp=n_tp),
         out_shape=(
-            jax.ShapeDtypeStruct((length // n_tp, features), BF16),
-            jax.ShapeDtypeStruct((count, features), BF16),
+            VMEM((length // n_tp, features), BF16),
+            VMEM((count, features), BF16),
         ),
         in_specs=[ANYWHERE] * len(operands),
         out_specs=(WHOLE, WHOLE),

time: 187 us -> 186 us (level)
  no operation moved by 1% of the time
where the time goes in v4:
time: 186 us
  Pallas kernels  184 us (99%)
    pallas_call x1, Pallas kernels, body(): pl.pallas_call(functools.partial(kernel, n_ep=n_ep, n_tp=n_tp), out_shape...  184 us

profile of v4, /device:TPU:33, one launch (start us, length us, event | category | flops | bytes accessed | tf_op | source)
XLA Modules:
  0.0 186.0 jit_solution(14963944963694389848)
XLA Ops:
  0.6 183.6 %whole.1 = (bf16[256,2048]{1,0:T(8,128)(2,1)S(1)}, bf16[128,2048]{1,0:T(8,128)(2,1)S(1)}) custom-call(bf16[1024,256]{1,0:T(8,128)(2,1)} %query.1, bf16[1024,256]{1,0:T(8,128)(2,1)} %gates.1, bf16[1024,256]{1,0:T(8,128)(2,1)} %value.1, f32[2,256]{1,0:T(2,128)} %margin.1, f32[2,1024]{1,0:T(2,128)} %position.1, f32[1,128]{1,0:T(1,128)} %bitcast.7, ...), custom_call_target="tpu_custom_call" | custom-call | tf_op jit(solution)/shard_map/whole/pallas_call | solution.py:810
  184.2 1.0 copy.18
  185.2 0.8 copy.19

commit v5 on v4

--- a/solution.py
+++ b/solution.py
@@ -238,7 +238,7 @@
     w_all, qin, kin, before, off, inc, last, fin, near, far, group_state, chip_in, entering,
     heads_out, heads_in, send, rows, parts, relay_l, relay_r, from_l, from_r, total, ret,
     xt, perm, lhs, early, lead, ahead_state,
-    in_sem, zs, zr, xs, xr_l, xr_r, ys, yr, qs, qr, fs, fr, ts, tr,
+    ready, in_sem, zs, zr, xs, xr_l, xr_r, ys, yr, qs, qr, fs, fr, ts, tr,
     mate_s, mate_r, near_s, near_r, far_s, far_r, lead_s, lead_r, chip_s, chip_r,
     ws, wr, wys, wyr, wms, wmr, hs, hr,
     *, n_ep, n_tp,
@@ -275,19 +275,30 @@
 
     barrier = pltpu.get_barrier_semaphore()
 
-    def greet(j, carry):
-        pl.semaphore_signal(
-            barrier, inc=1, device_id={"ep": (me + j) % n_ep}, device_id_type=MESH
-        )
+    def greet(e, carry):
+        @pl.when(e // 2 > z)
+        def _():
+            pl.semaphore_signal(barrier, inc=1, device_id={"ep": e}, device_id_type=MESH)
+
         return carry
 
-    lax.fori_loop(1, n_ep, greet, 0)
+    lax.fori_loop(0, n_ep, greet, 0)
+    pl.semaphore_signal(barrier, inc=1, device_id={"ep": mate}, device_id_type=MESH)
     for other in (left, right, opposite):
         pl.semaphore_signal(barrier, inc=1, device_id={"tp": other}, device_id_type=MESH)
     for copy in loads[:4]:
         copy.wait()
     pack_rows(tok_v, egain_v, routes_v, send)
-    pl.semaphore_wait(barrier, n_ep + n_tp - 2)
+    pl.semaphore_wait(barrier, 2 * z + n_tp)
+
+    def announce(e, carry):
+        @pl.when(e // 2 < z)
+        def _():
+            pl.semaphore_signal(ready.at[me], inc=1, device_id={"ep": e}, device_id_type=MESH)
+
+        return carry
+
+    lax.fori_loop(0, n_ep, announce, 0)
 
     def z_copy(b, side, core):
         other = ((z + offset(b, side)) % n_z) * 2 + core
@@ -306,19 +317,42 @@
     def is_self(b, side, core):
         return jnp.logical_and(jnp.logical_and(b == self_step, side == 0), core == c)
 
-    def dispatch(b, carry):
+    def dispatch_before(b, carry):
         for side in range(2):
             for core in range(2):
                 own = is_self(b, side, core)
+                chip = (z + offset(b, side)) % n_z
 
                 @pl.when(own)
                 def _():
                     own_in(4 * b + 2 * side + c).start()
 
-                @pl.when(jnp.logical_not(own))
+                @pl.when(jnp.logical_and(chip <= z, jnp.logical_not(own)))
                 def _():
                     z_copy(b, side, core).start()
 
+        return carry
+
+    def dispatch_after(b, lowest, highest):
+        for side in range(2):
+            for core in range(2):
+                chip = (z + offset(b, side)) % n_z
+
+                @pl.when(jnp.logical_and(chip >= z + lowest, chip <= z + highest))
+                def _():
+                    pl.semaphore_wait(ready.at[2 * chip + core], 1)
+                    z_copy(b, side, core).start()
+
+    def dispatch(b):
+        dispatch_before(b, 0)
+        dispatch_after(b, 1, n_z)
+
+    def soon(b, carry):
+        dispatch_after(b, 1, 3)
+        return carry
+
+    def later(b, carry):
+        dispatch_after(b, 4, n_z)
         return carry
 
     def x_copy(b, way):
@@ -652,7 +686,8 @@
         return 2 * other + core
 
     ahead = 4
-    lax.fori_loop(0, ahead, dispatch, 0)
+    lax.fori_loop(0, ahead, dispatch_before, 0)
+    lax.fori_loop(0, ahead, soon, 0)
     for copy in loads[4:]:
         copy.wait()
     w_copy(0).start()
@@ -666,6 +701,7 @@
     perm[...] = jnp.where(col == target, 1.0, 0.0).astype(BF16)
     recurrence_states(q_v, g_v, v_v, margin_v, pos_v, qin, kin, before, off, fin, inc, last)
     mate_copy().start()
+    lax.fori_loop(0, ahead, later, 0)
 
     def body(i, carry):
         def stage(lag, fn, until=steps):
@@ -700,10 +736,10 @@
         stage(0, arrive)
         once(0, send_chip)
         once(1, relay_weights)
+        stage(0, lambda b: dispatch(b + ahead), steps - ahead)
         once(3, share_group)
-        stage(0, lambda b: dispatch(b + ahead, 0), steps - ahead)
         once(4, pair_weights)
-        once(6, share_far)
+        once(7, share_far)
         return carry
 
     lax.fori_loop(0, steps + 4, body, 0)
@@ -834,6 +870,7 @@
             VMEM((2 * QUARTERS * count, n_ep * chunk), BF16),
             VMEM((2 * QUARTERS * count, width), F32),
             VMEM((2, HC, HC), BF16), VMEM((2, HC, HC), F32),
+            pltpu.SemaphoreType.REGULAR((n_ep,)),
             dma((len(operands),)),
             dma((n_ep,)), dma((n_ep,)),
             dma((2, steps)), dma((steps,)), dma((steps,)),

time: 186 us -> 190 us (1.022); the launches traced: 186 us -> 187 us
  no operation moved by 1% of the time
where the time goes in v5:
time: 190 us; the launch traced here: 187 us
  Pallas kernels  185 us (97%)
    pallas_call x1, Pallas kernels, body(): pl.pallas_call(functools.partial(kernel, n_ep=n_ep, n_tp=n_tp), out_shape...  185 us

profile of v5, /device:TPU:33, one launch (start us, length us, event | category | flops | bytes accessed | tf_op | source)
XLA Modules:
  0.0 187.5 jit_solution(15337103895773479934)
XLA Ops:
  0.6 185.0 %whole.1 = (bf16[256,2048]{1,0:T(8,128)(2,1)S(1)}, bf16[128,2048]{1,0:T(8,128)(2,1)S(1)}) custom-call(bf16[1024,256]{1,0:T(8,128)(2,1)} %query.1, bf16[1024,256]{1,0:T(8,128)(2,1)} %gates.1, bf16[1024,256]{1,0:T(8,128)(2,1)} %value.1, f32[2,256]{1,0:T(2,128)} %margin.1, f32[2,1024]{1,0:T(2,128)} %position.1, f32[1,128]{1,0:T(1,128)} %bitcast.7, ...), custom_call_target="tpu_custom_call" | custom-call | tf_op jit(solution)/shard_map/whole/pallas_call | solution.py:846
  185.7 1.0 copy.18
  186.7 0.8 copy.19

commit v6 on v4

--- a/solution.py
+++ b/solution.py
@@ -270,7 +270,7 @@
             )
         )
     ]
-    for copy in loads:
+    for copy in loads[:3]:
         copy.start()
 
     barrier = pltpu.get_barrier_semaphore()
@@ -284,8 +284,10 @@
     lax.fori_loop(1, n_ep, greet, 0)
     for other in (left, right, opposite):
         pl.semaphore_signal(barrier, inc=1, device_id={"tp": other}, device_id_type=MESH)
-    for copy in loads[:4]:
+    for copy in loads[:3]:
         copy.wait()
+    for copy in loads[3:]:
+        copy.start()
     pack_rows(tok_v, egain_v, routes_v, send)
     pl.semaphore_wait(barrier, n_ep + n_tp - 2)
 
@@ -653,7 +655,7 @@
 
     ahead = 4
     lax.fori_loop(0, ahead, dispatch, 0)
-    for copy in loads[4:]:
+    for copy in loads[3:]:
         copy.wait()
     w_copy(0).start()
     w_copy(1).start()

time: 186 us -> 187 us (level)
  no operation moved by 1% of the time
where the time goes in v6:
time: 187 us
  Pallas kernels  184 us (98%)
    pallas_call x1, Pallas kernels, body(): pl.pallas_call(functools.partial(kernel, n_ep=n_ep, n_tp=n_tp), out_shape...  184 us

profile of v6, /device:TPU:33, one launch (start us, length us, event | category | flops | bytes accessed | tf_op | source)
XLA Modules:
  0.0 186.9 jit_solution(5240699812295182996)
XLA Ops:
  0.6 184.5 %whole.1 = (bf16[256,2048]{1,0:T(8,128)(2,1)S(1)}, bf16[128,2048]{1,0:T(8,128)(2,1)S(1)}) custom-call(bf16[1024,256]{1,0:T(8,128)(2,1)} %query.1, bf16[1024,256]{1,0:T(8,128)(2,1)} %gates.1, bf16[1024,256]{1,0:T(8,128)(2,1)} %value.1, f32[2,256]{1,0:T(2,128)} %margin.1, f32[2,1024]{1,0:T(2,128)} %position.1, f32[1,128]{1,0:T(1,128)} %bitcast.7, ...), custom_call_target="tpu_custom_call" | custom-call | tf_op jit(solution)/shard_map/whole/pallas_call | solution.py:812
  185.1 1.0 copy.18
  186.1 0.8 copy.19
